TPU v7x, 32 devices: a whole 2x2x4 slice. The times are simulated.
32 devices in a mesh: st: 4 (over y, x), tp: 8 (over z, core).
Axes of the slice: x: 2, y: 2, z: 4, core: 2. Of those that a mesh axis runs over, the one named last changes fastest.
Arguments:
- tokens: bfloat16 [2048, 4096], P('st', 'tp'), may hold values from -6 to 6
- w_query: bfloat16 [4096, 2048], P(None, 'tp'), may hold values from -0.09375 to 0.09375
- w_key: bfloat16 [4096, 2048], P(None, 'tp'), may hold values from -0.09375 to 0.09375
- w_value: bfloat16 [4096, 4096], P(None, 'tp'), may hold values from -0.09375 to 0.09375
- w_mem_query: bfloat16 [4096, 2048], P(None, 'tp'), may hold values from -0.09375 to 0.09375
- w_mem_key: bfloat16 [4096, 2048], P(None, 'tp'), may hold values from -0.09375 to 0.09375
- w_mem_value: bfloat16 [4096, 2048], P(None, 'tp'), may hold values from -0.09375 to 0.09375
- w_gate: bfloat16 [4096, 16], P(None, 'tp'), may hold values from -0.09375 to 0.09375
- w_lift: bfloat16 [16, 128, 256], P('tp'), may hold values from -4 to 4
- decay_rate: float32 [16], P('tp'), may hold values from 0.000390625 to 0.1
- store: bfloat16 [512, 64, 4096], P('st', None, 'tp'), may hold values from -6 to 6
- passage_ids: int32 [16, 2], P('st'), may hold values from 0 to 511, as said below
Outputs:
- mixed: bfloat16 [2048, 4096], P('st', 'tp')
Inputs may be any that keep to these rules, and one draw needn't show every extreme that they name: `passage_ids`: passage p is held by index p // 128 of st. Among the requests of the rows of one device along st, at most 4 name passages held by one index of st, and in every draw some index receives exactly 4 of them.
All inputs are finite; a program needn't handle non-finite values.
Results may differ from a plain program's by a relative error of at most 0.0095.
Values may be sent and summed in bfloat16 or wider, within the bound.
No kernel may reach another device: no remote copies, remote signals or barrier semaphores. Data moves between devices by JAX's collectives and lax.ppermute only.
A program may use at most 64 MiB of HBM per device.

v0:
```python
import functools

import jax
import jax.numpy as jnp
from jax import lax
from jax.experimental import pallas as pl
from jax.experimental.pallas import tpu as pltpu
from jax.sharding import PartitionSpec as P


D = 4096
KEY_DIM = 128
VALUE_DIM = 256
MEM_DIM = 128
SEQ_LEN = 512
BLOCK = 128
PASS_ROWS = 64
LANES = 128
TILE = 128

norm_eps = 1e-06
rope_base = 10000.0


f32 = jnp.float32
bf16 = jnp.bfloat16
ANY = pl.BlockSpec(memory_space=pl.ANY)
SMEM = pl.BlockSpec(memory_space=pltpu.SMEM)
VMEM = pl.BlockSpec(memory_space=pltpu.VMEM)


def rotary_tables(rows):
    half_dim = KEY_DIM // 2
    positions = (jnp.arange(rows, dtype=jnp.int32) % SEQ_LEN).astype(f32)
    inverse = rope_base ** (-jnp.arange(half_dim, dtype=f32) / half_dim)
    angles = positions[:, None] * inverse[None, :]
    cosine = jnp.cos(angles)
    sine = jnp.sin(angles)
    return (
        jnp.concatenate([cosine, cosine], axis=1),
        jnp.concatenate([-sine, sine], axis=1),
    )


def dot(a, b):
    return jnp.dot(a, b, preferred_element_type=f32)


def ring_gather(halves, ring_size, core_count):
    total = ring_size * core_count
    half = halves[0].shape[0]
    me = lax.axis_index("tp")

    def step(value, chips):
        moves = [(i, (i + chips * core_count) % total) for i in range(total)]
        return lax.ppermute(value, "tp", moves)

    def swap(value):
        moves = [(i, i + 1 - 2 * (i % 2)) for i in range(total)]
        return lax.ppermute(value, "tp", moves)

    held = [(halves[0], 0, 0), (halves[1], 0, half)]
    right = left = halves
    far = ring_size // 2
    for distance in range(1, far):
        right_top, left_bottom = step(right[0], 1), step(left[1], -1)
        right_bottom, left_top = step(right[1], 1), step(left[0], -1)
        right, left = (right_top, right_bottom), (left_top, left_bottom)
        held += [
            (right_top, -distance, 0),
            (left_bottom, distance, half),
            (right_bottom, -distance, half),
            (left_top, distance, 0),
        ]
    if ring_size > 1:
        held += [(step(right[0], 1), far, 0), (step(left[1], -1), far, half)]
    parts = []
    chips = []
    for value, offset, first in held:
        offset = offset % ring_size
        if offset not in chips:
            chips.append(offset)
        slot = chips.index(offset) * core_count
        parts.append((value, slot, first))
        parts.append((swap(value), slot + 1, first))
    order = []
    core = me & 1
    for offset in chips:
        base = ((me >> 1) + offset) & (ring_size - 1)
        order += [base * core_count + core, base * core_count + 1 - core]
    return parts, jnp.stack(order)


def project_kernel(places, heads, *refs):
    count = len(places)
    order, rates = refs[:2]
    parts = refs[2 : 2 + count]
    weights = refs[2 + count : 7 + count]
    cos_ref, sin_ref, norm_out, query_out, gate_out, xs, ws, acc, sem_x, sem_w = refs[7 + count :]
    slots = ws.shape[0]
    depth = ws.shape[1]
    rows = xs.shape[1]
    copies = [[] for _ in range(slots)]
    for p, (slot, first) in enumerate(places):
        extent = parts[p].shape[0]
        copies[slot].append(
            pltpu.make_async_copy(parts[p], xs.at[slot, pl.ds(first, extent)], sem_x.at[p])
        )
    for slot in range(slots):
        start = 0
        row = pl.multiple_of(order[slot] * depth, depth)
        for w, weight in enumerate(weights):
            width = weight.shape[1]
            copies[slot].append(
                pltpu.make_async_copy(
                    weight.at[pl.ds(row, depth)],
                    ws.at[slot, :, pl.ds(start, width)],
                    sem_w.at[slot, w],
                )
            )
            start += width
    for group in copies:
        for copy in group:
            copy.start()
    squares = jnp.zeros((rows, LANES), f32)
    for slot in range(slots):
        for copy in copies[slot]:
            copy.wait()
        x = xs[slot]
        wide = x.astype(f32)
        wide = wide * wide
        for lane in range(depth // LANES):
            squares += wide[:, lane * LANES : (lane + 1) * LANES]
        if slot == 0:
            acc[...] = dot(x, ws[slot])
        else:
            acc[...] += dot(x, ws[slot])
    row_scale = lax.rsqrt(jnp.sum(squares, axis=1, keepdims=True) / D + norm_eps)
    key_at = heads * KEY_DIM
    value_at = 2 * heads * KEY_DIM
    mem_at = value_at + heads * VALUE_DIM
    gate_at = mem_at + heads * MEM_DIM
    gate_raw = acc[:, gate_at : gate_at + LANES] * row_scale
    gate_out[...] = jax.nn.sigmoid(gate_raw)
    cosine = cos_ref[...]
    sine = sin_ref[...]
    for h in range(heads):
        z = acc[:, mem_at + h * MEM_DIM : mem_at + (h + 1) * MEM_DIM]
        z = z * lax.rsqrt(jnp.mean(z * z, axis=1, keepdims=True) + norm_eps)
        query_out[:, h * MEM_DIM : (h + 1) * MEM_DIM] = z.astype(bf16)
        q = acc[:, h * KEY_DIM : (h + 1) * KEY_DIM] * row_scale
        q = (q * cosine + pltpu.roll(q, KEY_DIM // 2, 1) * sine).astype(bf16)
        k = acc[:, key_at + h * KEY_DIM : key_at + (h + 1) * KEY_DIM] * row_scale
        k = (k * cosine + pltpu.roll(k, KEY_DIM // 2, 1) * sine) * KEY_DIM ** (-0.5)
        k = k.astype(bf16)
        v = acc[:, value_at + h * VALUE_DIM : value_at + (h + 1) * VALUE_DIM] * row_scale
        v = v.astype(bf16)
        for first in range(0, rows, TILE):
            base = first // SEQ_LEN * SEQ_LEN
            end = first + TILE
            scores = lax.dot_general(
                q[first:end], k[base:end], (((1,), (1,)), ((), ())), preferred_element_type=f32
            )
            shape = scores.shape
            gap = (
                lax.broadcasted_iota(jnp.int32, shape, 0)
                - lax.broadcasted_iota(jnp.int32, shape, 1)
                + (first - base)
            )
            decay = jnp.exp(-rates[h] * jnp.maximum(gap, 0).astype(f32))
            scores = jnp.where(gap >= 0, scores * decay, 0.0)
            upper = scores.astype(bf16)
            lower = (scores - upper.astype(f32)).astype(bf16)
            out = dot(upper, v[base:end]) + dot(lower, v[base:end])
            out = out - jnp.mean(out, axis=1, keepdims=True)
            out = out * lax.rsqrt(jnp.mean(out * out, axis=1, keepdims=True) + norm_eps)
            norm_out[first:end, h * VALUE_DIM : (h + 1) * VALUE_DIM] = out


def project(parts, order, weights, rates, tables):
    heads = rates.shape[0]
    places = tuple((slot, first) for _, slot, first in parts)
    rows, depth = 2 * parts[0][0].shape[0], parts[0][0].shape[1]
    slots = order.shape[0]
    width = sum(w.shape[1] for w in weights)
    return pl.pallas_call(
        functools.partial(project_kernel, places, heads),
        out_shape=(
            jax.ShapeDtypeStruct((rows, heads * VALUE_DIM), f32),
            jax.ShapeDtypeStruct((rows, heads * MEM_DIM), bf16),
            jax.ShapeDtypeStruct((rows, LANES), f32),
        ),
        in_specs=[SMEM, SMEM] + [ANY] * (len(parts) + len(weights)) + [VMEM, VMEM],
        out_specs=(VMEM, VMEM, VMEM),
        scratch_shapes=[
            pltpu.VMEM((slots, rows, depth), bf16),
            pltpu.VMEM((slots, depth, width), bf16),
            pltpu.VMEM((rows, width), f32),
            pltpu.SemaphoreType.DMA((len(parts),)),
            pltpu.SemaphoreType.DMA((slots, len(weights))),
        ],
        compiler_params=pltpu.CompilerParams(vmem_limit_bytes=40 * 1024 * 1024),
        cost_estimate=pl.CostEstimate(
            flops=2 * rows * depth * slots * width, bytes_accessed=0, transcendentals=0
        ),
        name="project_retain",
    )(order, rates, *[p[0] for p in parts], *weights, *tables)


def fetch_kernel(index, store, *refs):
    outs, sems = refs[:-1], refs[-1]
    copies = []
    for out in outs:
        for i in range(out.shape[0]):
            at = len(copies)
            copies.append(pltpu.make_async_copy(store.at[index[at]], out.at[i], sems.at[at]))
    for copy in copies:
        copy.start()
    for copy in copies:
        copy.wait()


def fetch(store, index, peers):
    count = index.shape[0]
    shape = jax.ShapeDtypeStruct((count // peers,) + store.shape[1:], store.dtype)
    return pl.pallas_call(
        fetch_kernel,
        out_shape=(shape,) * peers,
        in_specs=[SMEM, ANY],
        out_specs=(VMEM,) * peers,
        scratch_shapes=[pltpu.SemaphoreType.DMA((count,))],
        name="fetch_rows",
    )(index, store)


def compact_kernel(source, index, store, *refs):
    arrived = refs[:-3]
    halves, sems = refs[-3:-1], refs[-1]
    half = halves[0].shape[0]
    for i in range(2 * half):
        out = halves[i // half].at[i % half]
        for k, ref in enumerate((store,) + tuple(arrived)):

            @pl.when(source[i] == k)
            def _():
                pltpu.make_async_copy(ref.at[index[i]], out, sems.at[i]).start()

    for i in range(2 * half):
        out = halves[i // half].at[i % half]
        pltpu.make_async_copy(store.at[0], out, sems.at[i]).wait()


def compact(store, arrived, source, index):
    count = index.shape[0]
    shape = jax.ShapeDtypeStruct((count // 2,) + store.shape[1:], store.dtype)
    return pl.pallas_call(
        compact_kernel,
        out_shape=(shape, shape),
        in_specs=[SMEM, SMEM] + [ANY] * (1 + len(arrived)),
        out_specs=(VMEM, VMEM),
        scratch_shapes=[pltpu.SemaphoreType.DMA((count,))],
        name="compact_rows",
    )(source, index, store, *arrived)


def passage_kernel(places, heads, picks, *refs):
    count = len(places)
    order = refs[0]
    parts = refs[1 : 1 + count]
    weights = refs[1 + count : 3 + count]
    query, gate, norm, lift, out, xs, ws, acc, sem_x, sem_w = refs[3 + count :]
    slots = ws.shape[0]
    depth = ws.shape[1]
    width = heads * MEM_DIM
    copies = [[] for _ in range(slots)]
    for p, (slot, first) in enumerate(places):
        extent = parts[p].shape[0]
        copies[slot].append(
            pltpu.make_async_copy(parts[p], xs.at[slot, pl.ds(first, extent)], sem_x.at[p])
        )
    for slot in range(slots):
        row = pl.multiple_of(order[slot] * depth, depth)
        for w, weight in enumerate(weights):
            copies[slot].append(
                pltpu.make_async_copy(
                    weight.at[pl.ds(row, depth)],
                    ws.at[slot, :, pl.ds(w * width, width)],
                    sem_w.at[slot, w],
                )
            )
    for group in copies:
        for copy in group:
            copy.start()
    for slot in range(slots):
        for copy in copies[slot]:
            copy.wait()
        if slot == 0:
            acc[...] = dot(xs[slot], ws[slot])
        else:
            acc[...] += dot(xs[slot], ws[slot])
    block_rows = picks * PASS_ROWS
    for h in range(heads):
        lo, hi = h * MEM_DIM, (h + 1) * MEM_DIM
        k = acc[:, lo:hi]
        k = k * lax.rsqrt(jnp.mean(k * k, axis=1, keepdims=True) + norm_eps)
        k = k.astype(bf16)
        v = acc[:, width + lo : width + hi].astype(bf16)
        for b in range(query.shape[0] // BLOCK):
            top, end = b * BLOCK, (b + 1) * BLOCK
            q = query[top:end, lo:hi]
            first, last = b * block_rows, (b + 1) * block_rows
            scores = lax.dot_general(
                q, k[first:last], (((1,), (1,)), ((), ())), preferred_element_type=f32
            )
            exponent = jnp.exp(scores * MEM_DIM ** (-0.5))
            mass = jnp.sum(exponent, axis=1, keepdims=True)
            summed = dot(exponent.astype(bf16), v[first:last])
            mem_out = (summed / mass).astype(bf16)
            lifted = dot(mem_out, lift[h])
            cols = slice(h * VALUE_DIM, (h + 1) * VALUE_DIM)
            out[top:end, cols] = (
                norm[top:end, cols] + gate[top:end, h : h + 1] * lifted
            ).astype(bf16)


def passages(parts, order, weights, query, gate, norm, lift, picks):
    heads = lift.shape[0]
    places = tuple((slot, first) for _, slot, first in parts)
    rows, depth = 2 * parts[0][0].shape[0], parts[0][0].shape[1]
    slots = order.shape[0]
    width = sum(w.shape[1] for w in weights)
    return pl.pallas_call(
        functools.partial(passage_kernel, places, heads, picks),
        out_shape=jax.ShapeDtypeStruct(norm.shape, bf16),
        in_specs=[SMEM] + [ANY] * (len(parts) + len(weights)) + [VMEM] * 4,
        out_specs=VMEM,
        scratch_shapes=[
            pltpu.VMEM((slots, rows, depth), bf16),
            pltpu.VMEM((slots, depth, width), bf16),
            pltpu.VMEM((rows, width), f32),
            pltpu.SemaphoreType.DMA((len(parts),)),
            pltpu.SemaphoreType.DMA((slots, len(weights))),
        ],
        compiler_params=pltpu.CompilerParams(vmem_limit_bytes=32 * 1024 * 1024),
        cost_estimate=pl.CostEstimate(
            flops=2 * rows * depth * slots * width, bytes_accessed=0, transcendentals=0
        ),
        name="passage_mix",
    )(order, *[p[0] for p in parts], *weights, query, gate, norm, lift)


def per_device(
    ring_size,
    core_count,
    tokens,
    w_query,
    w_key,
    w_value,
    w_mem_query,
    w_mem_key,
    w_mem_value,
    w_gate,
    w_lift,
    decay_rate,
    store,
    passage_ids,
):
    block_count, picks = passage_ids.shape
    request_count = block_count * picks
    group_count = lax.axis_size("st")
    capacity = max(1, 2 * request_count // group_count)
    held_count = store.shape[0]
    mine = lax.axis_index("st")

    def exchange(value, k):
        return lax.ppermute(value, "st", [(i, i ^ k) for i in range(group_count)])

    wanted = passage_ids.reshape(request_count)
    owners = wanted // held_count
    held_index = wanted % held_count
    ordinal = jnp.arange(request_count, dtype=jnp.int32)
    earlier = (owners[:, None] == owners[None, :]) & (ordinal[None, :] < ordinal[:, None])
    slot_index = jnp.sum(earlier.astype(jnp.int32), axis=1)
    source = owners ^ mine
    place = source * capacity + slot_index
    selector = (
        place[:, None] == jnp.arange(group_count * capacity, dtype=jnp.int32)[None, :]
    ).astype(jnp.int32)
    outgoing = jnp.sum(selector * held_index[:, None], axis=0).reshape(group_count, capacity)
    incoming = [exchange(outgoing[k], k) for k in range(1, group_count)]

    half = tokens.shape[0] // 2
    token_halves = (tokens[:half], tokens[half:])
    token_parts, order = ring_gather(token_halves, ring_size, core_count)

    fetched = fetch(store, jnp.concatenate(incoming), group_count - 1)
    arrived = [exchange(fetched[k - 1], k) for k in range(1, group_count)]
    rows_at = jnp.where(source == 0, held_index, slot_index)
    own_rows = compact(store, arrived, source, rows_at)
    own_rows = [x.reshape(-1, store.shape[2]) for x in own_rows]
    row_parts, _ = ring_gather(tuple(own_rows), ring_size, core_count)

    gate_wide = jnp.pad(w_gate, ((0, 0), (0, LANES - w_gate.shape[1])))
    tables = rotary_tables(tokens.shape[0])
    norm, query, gate = project(
        token_parts,
        order,
        (w_query, w_key, w_value, w_mem_query, gate_wide),
        decay_rate,
        tables,
    )
    return passages(
        row_parts, order, (w_mem_key, w_mem_value), query, gate, norm, w_lift, picks
    )


def solution(mesh):
    in_specs = (
        P("st", "tp"),
        P(None, "tp"),
        P(None, "tp"),
        P(None, "tp"),
        P(None, "tp"),
        P(None, "tp"),
        P(None, "tp"),
        P(None, "tp"),
        P("tp", None, None),
        P("tp"),
        P("st", None, "tp"),
        P("st", None),
    )
    out_specs = P("st", "tp")
    core_count = 2
    ring_size = mesh.shape["tp"] // core_count
    body = functools.partial(per_device, ring_size, core_count)

    return jax.shard_map(
        body,
        mesh=mesh,
        in_specs=in_specs,
        out_specs=out_specs,
        check_vma=False,
    )
```

profile of v0, /device:TPU:0, one launch (start us, length us, event | category | flops | bytes accessed | tf_op | source)
XLA Modules:
  0.0 121.4 jit_solution(9049222808028462028)
XLA Ops:
  0.0 1.1 fusion.6
  1.1 5.1 %collective-permute-start.24 = (bf16[256,512]{1,0:T(8,128)(2,1)S(1)}, bf16[256,512]{1,0:T(8,128)(2,1)S(1)}, u32[]{:S(2)}, u32[]{:S(2)}) collective-permute-start(bf16[256,512]{1,0:T(8,128)(2,1)S(1)} %get-tuple-element.25.refs_4_), channel_id=1, source_target_pairs={{0,6},{1,7},{2,0},{3,1},{4,2},{5,3},{6,4},{7,5},{8,14},{9,15},{10,... | collective-permute-start | bytes 786440 | tf_op jit(solution)/shard_map/ppermute | solution.py:56
  6.2 0.8 copy.17
  7.3 0.5 compare_select_fusion
  7.9 1.5 %collective-permute-start = (s32[4]{0:T(128)S(1)}, s32[4]{0:T(128)S(1)}, u32[]{:S(2)}, u32[]{:S(2)}) collective-permute-start(s32[4]{0:T(128)S(1)} %get-tuple-element.30), channel_id=1, source_target_pairs={{0,8},{8,0},{16,24},{24,16},{1,9},{9,1},{17,25},{25,17},{2,10},{10... | collective-permute-start | bytes 56 | tf_op jit(solution)/shard_map/ppermute | solution.py:376
  9.4 1.5 %collective-permute-start.1 = (s32[4]{0:T(128)S(1)}, s32[4]{0:T(128)S(1)}, u32[]{:S(2)}, u32[]{:S(2)}) collective-permute-start(s32[4]{0:T(128)S(1)} %get-tuple-element.32), channel_id=1, source_target_pairs={{0,16},{8,24},{16,0},{24,8},{1,17},{9,25},{17,1},{25,9},{2,18},{10... | collective-permute-start | bytes 56 | tf_op jit(solution)/shard_map/ppermute | solution.py:376
  10.9 0.6 collective-permute-done
  11.5 2.4 %collective-permute-start.2 = (s32[4]{0:T(128)S(1)}, s32[4]{0:T(128)S(1)}, u32[]{:S(2)}, u32[]{:S(2)}) collective-permute-start(s32[4]{0:T(128)S(1)} %get-tuple-element.31), channel_id=1, source_target_pairs={{0,24},{8,16},{16,8},{24,0},{1,25},{9,17},{17,9},{25,1},{2,26},{10... | collective-permute-start | bytes 56 | tf_op jit(solution)/shard_map/ppermute | solution.py:376
  14.0 2.0 %collective-permute-done.2 = s32[4]{0:T(128)S(1)} collective-permute-done((s32[4]{0:T(128)S(1)}, s32[4]{0:T(128)S(1)}, u32[]{:S(2)}, u32[]{:S(2)}) %collective-permute-start.2) | collective-permute-done | bytes 48 | tf_op jit(solution)/shard_map/ppermute | solution.py:376
  16.0 0.6 pad_add_fusion.index
  16.6 2.8 %fetch_rows.1 = (bf16[4,64,512]{2,1,0:T(8,128)(2,1)}, bf16[4,64,512]{2,1,0:T(8,128)(2,1)}, bf16[4,64,512]{2,1,0:T(8,128)(2,1)}) custom-call(s32[12]{0:T(128)} %pad_add_fusion.index, bf16[128,64,512]{2,1,0:T(8,128)(2,1)} %store.3), custom_call_target="tpu_custom_call" | custom-call | tf_op jit(solution)/shard_map/fetch_rows/pallas_call | solution.py:226
  19.4 1.6 %collective-permute-start.3 = (bf16[4,64,512]{2,1,0:T(8,128)(2,1)}, bf16[4,64,512]{2,1,0:T(8,128)(2,1)S(1)}, u32[]{:S(2)}, u32[]{:S(2)}) collective-permute-start(bf16[4,64,512]{2,1,0:T(8,128)(2,1)} %get-tuple-element.13), channel_id=1, source_target_pairs={{0,8},{8,0},{16,24},{24,16},{1,9},{9,1},{17,25},{25,17},{2,10},{10... | collective-permute-start | bytes 786440 | tf_op jit(solution)/shard_map/ppermute | solution.py:376
  21.0 1.5 %collective-permute-start.4 = (bf16[4,64,512]{2,1,0:T(8,128)(2,1)}, bf16[4,64,512]{2,1,0:T(8,128)(2,1)S(1)}, u32[]{:S(2)}, u32[]{:S(2)}) collective-permute-start(bf16[4,64,512]{2,1,0:T(8,128)(2,1)} %get-tuple-element.14), channel_id=1, source_target_pairs={{0,16},{8,24},{16,0},{24,8},{1,17},{9,25},{17,1},{25,9},{2,18},{10... | collective-permute-start | bytes 786440 | tf_op jit(solution)/shard_map/ppermute | solution.py:376
  22.5 1.4 %collective-permute-done.22.refs_6_ = bf16[256,512]{1,0:T(8,128)(2,1)S(1)} collective-permute-done((bf16[256,512]{1,0:T(8,128)(2,1)S(1)}, bf16[256,512]{1,0:T(8,128)(2,1)S(1)}, u32[]{:S(2)}, u32[]{:S(2)}) %collective-permute-start.22) | collective-permute-done | bytes 262176 | tf_op jit(solution)/shard_map/ppermute | solution.py:56
  23.9 2.4 %collective-permute-start.5 = (bf16[4,64,512]{2,1,0:T(8,128)(2,1)}, bf16[4,64,512]{2,1,0:T(8,128)(2,1)S(1)}, u32[]{:S(2)}, u32[]{:S(2)}) collective-permute-start(bf16[4,64,512]{2,1,0:T(8,128)(2,1)} %get-tuple-element.15), channel_id=1, source_target_pairs={{0,24},{8,16},{16,8},{24,0},{1,25},{9,17},{17,9},{25,1},{2,26},{10... | collective-permute-start | bytes 786440 | tf_op jit(solution)/shard_map/ppermute | solution.py:376
  26.4 1.7 %collective-permute-start.28 = (bf16[256,512]{1,0:T(8,128)(2,1)S(1)}, bf16[256,512]{1,0:T(8,128)(2,1)S(1)}, u32[]{:S(2)}, u32[]{:S(2)}) collective-permute-start(bf16[256,512]{1,0:T(8,128)(2,1)S(1)} %get-tuple-element.26.refs_2_), channel_id=1, source_target_pairs={{0,6},{1,7},{2,0},{3,1},{4,2},{5,3},{6,4},{7,5},{8,14},{9,15},{10,... | collective-permute-start | bytes 786440 | tf_op jit(solution)/shard_map/ppermute | solution.py:56
  28.1 0.5 collective-permute-start.21
  28.6 4.6 %collective-permute-done.4.refs_1_ = bf16[4,64,512]{2,1,0:T(8,128)(2,1)S(1)} collective-permute-done((bf16[4,64,512]{2,1,0:T(8,128)(2,1)}, bf16[4,64,512]{2,1,0:T(8,128)(2,1)S(1)}, u32[]{:S(2)}, u32[]{:S(2)}) %collective-permute-start.4) | collective-permute-done | bytes 262176 | tf_op jit(solution)/shard_map/ppermute | solution.py:376
  33.2 1.6 %collective-permute-start.30 = (bf16[256,512]{1,0:T(8,128)(2,1)S(1)}, bf16[256,512]{1,0:T(8,128)(2,1)S(1)}, u32[]{:S(2)}, u32[]{:S(2)}) collective-permute-start(bf16[256,512]{1,0:T(8,128)(2,1)S(1)} %collective-permute-done.22.refs_6_), channel_id=1, source_target_pairs={{0,2},{1,3},{2,4},{3,5},{4,6},{5,7},{6,0},{7,1},{8,10},{9,11},{10,... | collective-permute-start | bytes 786440 | tf_op jit(solution)/shard_map/ppermute | solution.py:56
  34.8 2.3 %collective-permute-start.32 = (bf16[256,512]{1,0:T(8,128)(2,1)S(1)}, bf16[256,512]{1,0:T(8,128)(2,1)S(1)}, u32[]{:S(2)}, u32[]{:S(2)}) collective-permute-start(bf16[256,512]{1,0:T(8,128)(2,1)S(1)} %collective-permute-done.24.refs_8_), channel_id=1, source_target_pairs={{0,6},{1,7},{2,0},{3,1},{4,2},{5,3},{6,4},{7,5},{8,14},{9,15},{10,... | collective-permute-start | bytes 786440 | tf_op jit(solution)/shard_map/ppermute | solution.py:56
  37.1 2.8 %compact_rows.1 = (bf16[4,64,512]{2,1,0:T(8,128)(2,1)}, bf16[4,64,512]{2,1,0:T(8,128)(2,1)}) custom-call(s32[8]{0:T(128)} %copy-done.35, s32[8]{0:T(128)} %get-tuple-element.23.index, bf16[128,64,512]{2,1,0:T(8,128)(2,1)} %store.3, bf16[4,64,512]{2,1,0:T(8,128)(2,1)} %copy-done.31, bf16[4,64,512]{2,1,0:T(8,128)(2,1)} %copy-done.32, ...), custom_call_target="tpu_custom_call" | custom-call | tf_op jit(solution)/shard_map/compact_rows/pallas_call | solution.py:256
  39.9 0.7 copy-done.14
  40.6 0.5 collective-permute-start.25
  41.1 0.7 copy-done.16
  41.9 0.5 collective-permute-start.29
  42.4 0.7 copy-done.12
  43.0 1.5 %collective-permute-done.32.refs_16_ = bf16[256,512]{1,0:T(8,128)(2,1)S(1)} collective-permute-done((bf16[256,512]{1,0:T(8,128)(2,1)S(1)}, bf16[256,512]{1,0:T(8,128)(2,1)S(1)}, u32[]{:S(2)}, u32[]{:S(2)}) %collective-permute-start.32) | collective-permute-done | bytes 262176 | tf_op jit(solution)/shard_map/ppermute | solution.py:56
  44.5 2.5 %collective-permute-start.8 = (bf16[256,512]{1,0:T(8,128)(2,1)}, bf16[256,512]{1,0:T(8,128)(2,1)S(1)}, u32[]{:S(2)}, u32[]{:S(2)}) collective-permute-start(bf16[256,512]{1,0:T(8,128)(2,1)} %bitcast.10), channel_id=1, source_target_pairs={{0,2},{1,3},{2,4},{3,5},{4,6},{5,7},{6,0},{7,1},{8,10},{9,11},{10,... | collective-permute-start | bytes 786440 | tf_op jit(solution)/shard_map/ppermute | solution.py:56
  47.1 0.7 copy-done.22
  47.8 2.3 %collective-permute-start.10 = (bf16[256,512]{1,0:T(8,128)(2,1)}, bf16[256,512]{1,0:T(8,128)(2,1)S(1)}, u32[]{:S(2)}, u32[]{:S(2)}) collective-permute-start(bf16[256,512]{1,0:T(8,128)(2,1)} %bitcast.14), channel_id=1, source_target_pairs={{0,6},{1,7},{2,0},{3,1},{4,2},{5,3},{6,4},{7,5},{8,14},{9,15},{10,... | collective-permute-start | bytes 786440 | tf_op jit(solution)/shard_map/ppermute | solution.py:56
  50.0 0.7 copy-done.24
  50.7 0.2 collective-permute-start.12
  50.9 0.7 copy-done.26
  51.6 3.6 %collective-permute-start.14 = (bf16[256,512]{1,0:T(8,128)(2,1)}, bf16[256,512]{1,0:T(8,128)(2,1)S(1)}, u32[]{:S(2)}, u32[]{:S(2)}) collective-permute-start(bf16[256,512]{1,0:T(8,128)(2,1)} %bitcast.11), channel_id=1, source_target_pairs={{0,6},{1,7},{2,0},{3,1},{4,2},{5,3},{6,4},{7,5},{8,14},{9,15},{10,... | collective-permute-start | bytes 786440 | tf_op jit(solution)/shard_map/ppermute | solution.py:56
  55.3 0.7 copy-done.28
  56.0 0.7 collective-permute-done.8.refs_5_
  56.7 1.4 %copy.18 = bf16[4096,2]{1,0:T(8,128)(2,1)} copy(bf16[4096,2]{0,1:T(2,128)(2,1)S(1)} %copy-done.34) | data formatting | bytes 32768 | tf_op args[7]
  58.1 1.4 %pad.4.refs_22_ = bf16[4096,128]{1,0:T(8,128)(2,1)S(1)} pad(bf16[4096,2]{1,0:T(8,128)(2,1)} %copy.18, bf16[]{:T(256)} %constant.65.clone.1), padding=0_0x0_126 | pad | bytes 1064962 | tf_op jit(solution)/shard_map/jit(_pad)/pad | solution.py:403
  59.7 2.6 %collective-permute-done.10.refs_7_ = bf16[256,512]{1,0:T(8,128)(2,1)S(1)} collective-permute-done((bf16[256,512]{1,0:T(8,128)(2,1)}, bf16[256,512]{1,0:T(8,128)(2,1)S(1)}, u32[]{:S(2)}, u32[]{:S(2)}) %collective-permute-start.10) | collective-permute-done | bytes 262176 | tf_op jit(solution)/shard_map/ppermute | solution.py:56
  62.3 5.7 %collective-permute-done.12.refs_9_ = bf16[256,512]{1,0:T(8,128)(2,1)S(1)} collective-permute-done((bf16[256,512]{1,0:T(8,128)(2,1)}, bf16[256,512]{1,0:T(8,128)(2,1)S(1)}, u32[]{:S(2)}, u32[]{:S(2)}) %collective-permute-start.12) | collective-permute-done | bytes 262176 | tf_op jit(solution)/shard_map/ppermute | solution.py:56
  68.0 5.3 %collective-permute-done.14.refs_11_ = bf16[256,512]{1,0:T(8,128)(2,1)S(1)} collective-permute-done((bf16[256,512]{1,0:T(8,128)(2,1)}, bf16[256,512]{1,0:T(8,128)(2,1)S(1)}, u32[]{:S(2)}, u32[]{:S(2)}) %collective-permute-start.14) | collective-permute-done | bytes 262176 | tf_op jit(solution)/shard_map/ppermute | solution.py:56
  73.3 1.8 %collective-permute-start.18 = (bf16[256,512]{1,0:T(8,128)(2,1)S(1)}, bf16[256,512]{1,0:T(8,128)(2,1)S(1)}, u32[]{:S(2)}, u32[]{:S(2)}) collective-permute-start(bf16[256,512]{1,0:T(8,128)(2,1)S(1)} %collective-permute-done.10.refs_7_), channel_id=1, source_target_pairs={{0,6},{1,7},{2,0},{3,1},{4,2},{5,3},{6,4},{7,5},{8,14},{9,15},{10,... | collective-permute-start | bytes 786440 | tf_op jit(solution)/shard_map/ppermute | solution.py:56
  75.0 0.2 collective-permute-start.11
  75.4 1.0 fusion
  76.4 0.2 pad_maximum_fusion
  76.6 0.2 collective-permute-start.9
  76.8 0.3 collective-permute-start.13
  77.2 11.3 %collective-permute-done.16.refs_13_ = bf16[256,512]{1,0:T(8,128)(2,1)S(1)} collective-permute-done((bf16[256,512]{1,0:T(8,128)(2,1)S(1)}, bf16[256,512]{1,0:T(8,128)(2,1)S(1)}, u32[]{:S(2)}, u32[]{:S(2)}) %collective-permute-start.16) | collective-permute-done | bytes 262176 | tf_op jit(solution)/shard_map/ppermute | solution.py:56
  88.5 0.5 collective-permute-start.17
  89.1 1.6 %copy-done.6 = bf16[4096,256]{1,0:T(8,128)(2,1)S(1)} copy-done((bf16[4096,256]{1,0:T(8,128)(2,1)S(1)}, bf16[4096,256]{1,0:T(8,128)(2,1)}, u32[]{:S(2)}) %copy-start.6) | copy-done | bytes 2097176
  90.7 1.6 %copy-done.7 = bf16[4096,256]{1,0:T(8,128)(2,1)S(1)} copy-done((bf16[4096,256]{1,0:T(8,128)(2,1)S(1)}, bf16[4096,256]{1,0:T(8,128)(2,1)}, u32[]{:S(2)}) %copy-start.7) | copy-done | bytes 2097176
  92.3 0.9 copy-done.9
  93.2 0.9 copy-done.11
  94.2 0.9 copy-done.13
  95.1 0.9 copy-done.15
  96.1 0.9 copy-done.17
  97.0 0.9 copy-done.19
  98.0 0.9 copy-done.21
  98.9 0.9 copy-done.23
  99.9 0.9 copy-done.25
  100.8 0.9 copy-done.27
  101.8 0.9 copy-done.29
  102.8 11.9 %project_retain.1 = (f32[512,512]{1,0:T(8,128)S(1)}, bf16[512,256]{1,0:T(8,128)(2,1)S(1)}, f32[512,128]{1,0:T(8,128)S(1)}) custom-call(s32[8]{0:T(128)S(1)} %stack.35.refs_0_, f32[2]{0:T(128)S(1)} %copy-done.30, bf16[256,512]{1,0:T(8,128)(2,1)S(1)} %get-tuple-element.26.refs_2_, bf16[256,512]{1,0:T(8,128)(2,1)S(1)} %copy-done.15, ...), custom_call_target="tpu_custom_call" | custom-call | flops 5905580032 | tf_op jit(solution)/shard_map/project_retain/pallas_call | solution.py:186
  114.8 6.5 %passage_mix.1 = bf16[512,512]{1,0:T(8,128)(2,1)} custom-call(s32[8]{0:T(128)S(1)} %stack.35.refs_0_, bf16[256,512]{1,0:T(8,128)(2,1)S(1)} %bitcast.13, bf16[256,512]{1,0:T(8,128)(2,1)S(1)} %collective-permute-done.6.refs_2_, bf16[256,512]{1,0:T(8,128)(2,1)S(1)} %bitcast.17, bf16[256,512]{1,0:T(8,128)(2,1)S(1)} %collective-permute-done.7.refs_4_, ...), custom_call_target="tpu_custom_call" | custom-call | flops 2147483648 | tf_op jit(solution)/shard_map/passage_mix/pallas_call | solution.py:332
  (97 shorter events, 1.0 us)
Async XLA Ops:
  1.1 25.3 %collective-permute-start.24 = (bf16[256,512]{1,0:T(8,128)(2,1)S(1)}, bf16[256,512]{1,0:T(8,128)(2,1)S(1)}, u32[]{:S(2)}, u32[]{:S(2)}) collective-permute-start(bf16[256,512]{1,0:T(8,128)(2,1)S(1)} %get-tuple-element.25.refs_4_), channel_id=1, source_target_pairs={{0,6},{1,7},{2,0},{3,1},{4,2},{5,3},{6,4},{7,5},{8,14},{9,15},{10,... | collective-permute-start | bytes 786440 | tf_op jit(solution)/shard_map/ppermute | solution.py:56
  6.2 21.9 %collective-permute-start.26 = (bf16[256,512]{1,0:T(8,128)(2,1)S(1)}, bf16[256,512]{1,0:T(8,128)(2,1)S(1)}, u32[]{:S(2)}, u32[]{:S(2)}) collective-permute-start(bf16[256,512]{1,0:T(8,128)(2,1)S(1)} %get-tuple-element.25.refs_4_), channel_id=1, source_target_pairs={{0,2},{1,3},{2,4},{3,5},{4,6},{5,7},{6,0},{7,1},{8,10},{9,11},{10,... | collective-permute-start | bytes 786440 | tf_op jit(solution)/shard_map/ppermute | solution.py:56
  6.2 17.7 %collective-permute-start.22 = (bf16[256,512]{1,0:T(8,128)(2,1)S(1)}, bf16[256,512]{1,0:T(8,128)(2,1)S(1)}, u32[]{:S(2)}, u32[]{:S(2)}) collective-permute-start(bf16[256,512]{1,0:T(8,128)(2,1)S(1)} %get-tuple-element.26.refs_2_), channel_id=1, source_target_pairs={{0,2},{1,3},{2,4},{3,5},{4,6},{5,7},{6,0},{7,1},{8,10},{9,11},{10,... | collective-permute-start | bytes 786440 | tf_op jit(solution)/shard_map/ppermute | solution.py:56
  7.3 12.1 %copy-start.35 = (s32[8]{0:T(128)}, s32[8]{0:T(128)S(1)}, u32[]{:S(2)}) copy-start(s32[8]{0:T(128)S(1)} %get-tuple-element.22.source) | copy-start | bytes 100
  7.9 3.6 %collective-permute-start = (s32[4]{0:T(128)S(1)}, s32[4]{0:T(128)S(1)}, u32[]{:S(2)}, u32[]{:S(2)}) collective-permute-start(s32[4]{0:T(128)S(1)} %get-tuple-element.30), channel_id=1, source_target_pairs={{0,8},{8,0},{16,24},{24,16},{1,9},{9,1},{17,25},{25,17},{2,10},{10... | collective-permute-start | bytes 56 | tf_op jit(solution)/shard_map/ppermute | solution.py:376
  9.4 4.5 %collective-permute-start.1 = (s32[4]{0:T(128)S(1)}, s32[4]{0:T(128)S(1)}, u32[]{:S(2)}, u32[]{:S(2)}) collective-permute-start(s32[4]{0:T(128)S(1)} %get-tuple-element.32), channel_id=1, source_target_pairs={{0,16},{8,24},{16,0},{24,8},{1,17},{9,25},{17,1},{25,9},{2,18},{10... | collective-permute-start | bytes 56 | tf_op jit(solution)/shard_map/ppermute | solution.py:376
  11.5 4.5 %collective-permute-start.2 = (s32[4]{0:T(128)S(1)}, s32[4]{0:T(128)S(1)}, u32[]{:S(2)}, u32[]{:S(2)}) collective-permute-start(s32[4]{0:T(128)S(1)} %get-tuple-element.31), channel_id=1, source_target_pairs={{0,24},{8,16},{16,8},{24,0},{1,25},{9,17},{17,9},{25,1},{2,26},{10... | collective-permute-start | bytes 56 | tf_op jit(solution)/shard_map/ppermute | solution.py:376
  19.4 8.7 %collective-permute-start.3 = (bf16[4,64,512]{2,1,0:T(8,128)(2,1)}, bf16[4,64,512]{2,1,0:T(8,128)(2,1)S(1)}, u32[]{:S(2)}, u32[]{:S(2)}) collective-permute-start(bf16[4,64,512]{2,1,0:T(8,128)(2,1)} %get-tuple-element.13), channel_id=1, source_target_pairs={{0,8},{8,0},{16,24},{24,16},{1,9},{9,1},{17,25},{25,17},{2,10},{10... | collective-permute-start | bytes 786440 | tf_op jit(solution)/shard_map/ppermute | solution.py:376
  21.0 12.2 %collective-permute-start.4 = (bf16[4,64,512]{2,1,0:T(8,128)(2,1)}, bf16[4,64,512]{2,1,0:T(8,128)(2,1)S(1)}, u32[]{:S(2)}, u32[]{:S(2)}) collective-permute-start(bf16[4,64,512]{2,1,0:T(8,128)(2,1)} %get-tuple-element.14), channel_id=1, source_target_pairs={{0,16},{8,24},{16,0},{24,8},{1,17},{9,25},{17,1},{25,9},{2,18},{10... | collective-permute-start | bytes 786440 | tf_op jit(solution)/shard_map/ppermute | solution.py:376
  23.9 15.9 %copy-start.10 = (bf16[256,512]{1,0:T(8,128)(2,1)}, bf16[256,512]{1,0:T(8,128)(2,1)S(1)}, u32[]{:S(2)}) copy-start(bf16[256,512]{1,0:T(8,128)(2,1)S(1)} %collective-permute-done.22.refs_6_) | copy-start | bytes 786436
  23.9 10.9 %collective-permute-start.5 = (bf16[4,64,512]{2,1,0:T(8,128)(2,1)}, bf16[4,64,512]{2,1,0:T(8,128)(2,1)S(1)}, u32[]{:S(2)}, u32[]{:S(2)}) collective-permute-start(bf16[4,64,512]{2,1,0:T(8,128)(2,1)} %get-tuple-element.15), channel_id=1, source_target_pairs={{0,24},{8,16},{16,8},{24,0},{1,25},{9,17},{17,9},{25,1},{2,26},{10... | collective-permute-start | bytes 786440 | tf_op jit(solution)/shard_map/ppermute | solution.py:376
  26.4 13.5 %collective-permute-start.28 = (bf16[256,512]{1,0:T(8,128)(2,1)S(1)}, bf16[256,512]{1,0:T(8,128)(2,1)S(1)}, u32[]{:S(2)}, u32[]{:S(2)}) collective-permute-start(bf16[256,512]{1,0:T(8,128)(2,1)S(1)} %get-tuple-element.26.refs_2_), channel_id=1, source_target_pairs={{0,6},{1,7},{2,0},{3,1},{4,2},{5,3},{6,4},{7,5},{8,14},{9,15},{10,... | collective-permute-start | bytes 786440 | tf_op jit(solution)/shard_map/ppermute | solution.py:56
  28.1 13.0 %copy-start.8 = (bf16[256,512]{1,0:T(8,128)(2,1)}, bf16[256,512]{1,0:T(8,128)(2,1)S(1)}, u32[]{:S(2)}) copy-start(bf16[256,512]{1,0:T(8,128)(2,1)S(1)} %collective-permute-done.26.refs_10_) | copy-start | bytes 786436
  28.1 11.8 %collective-permute-start.20 = (bf16[256,512]{1,0:T(8,128)(2,1)S(1)}, bf16[256,512]{1,0:T(8,128)(2,1)S(1)}, u32[]{:S(2)}, u32[]{:S(2)}) collective-permute-start(bf16[256,512]{1,0:T(8,128)(2,1)S(1)} %get-tuple-element.26.refs_2_), channel_id=1, source_target_pairs={{0,1},{1,0},{2,3},{3,2},{4,5},{5,4},{6,7},{7,6},{8,9},{9,8},{10,11... | collective-permute-start | bytes 786440 | tf_op jit(solution)/shard_map/ppermute | solution.py:60
  28.1 8.9 %copy-start.31 = (bf16[4,64,512]{2,1,0:T(8,128)(2,1)}, bf16[4,64,512]{2,1,0:T(8,128)(2,1)S(1)}, u32[]{:S(2)}) copy-start(bf16[4,64,512]{2,1,0:T(8,128)(2,1)S(1)} %collective-permute-done.3.refs_0_) | copy-start | bytes 786436
  28.1 13.0 %collective-permute-start.21 = (bf16[256,512]{1,0:T(8,128)(2,1)S(1)}, bf16[256,512]{1,0:T(8,128)(2,1)S(1)}, u32[]{:S(2)}, u32[]{:S(2)}) collective-permute-start(bf16[256,512]{1,0:T(8,128)(2,1)S(1)} %get-tuple-element.25.refs_4_), channel_id=1, source_target_pairs={{0,1},{1,0},{2,3},{3,2},{4,5},{5,4},{6,7},{7,6},{8,9},{9,8},{10,11... | collective-permute-start | bytes 786440 | tf_op jit(solution)/shard_map/ppermute | solution.py:60
  33.2 3.8 %copy-start.32 = (bf16[4,64,512]{2,1,0:T(8,128)(2,1)}, bf16[4,64,512]{2,1,0:T(8,128)(2,1)S(1)}, u32[]{:S(2)}) copy-start(bf16[4,64,512]{2,1,0:T(8,128)(2,1)S(1)} %collective-permute-done.4.refs_1_) | copy-start | bytes 786436
  33.2 8.6 %collective-permute-start.30 = (bf16[256,512]{1,0:T(8,128)(2,1)S(1)}, bf16[256,512]{1,0:T(8,128)(2,1)S(1)}, u32[]{:S(2)}, u32[]{:S(2)}) collective-permute-start(bf16[256,512]{1,0:T(8,128)(2,1)S(1)} %collective-permute-done.22.refs_6_), channel_id=1, source_target_pairs={{0,2},{1,3},{2,4},{3,5},{4,6},{5,7},{6,0},{7,1},{8,10},{9,11},{10,... | collective-permute-start | bytes 786440 | tf_op jit(solution)/shard_map/ppermute | solution.py:56
  34.8 2.3 %copy-start.33 = (bf16[4,64,512]{2,1,0:T(8,128)(2,1)}, bf16[4,64,512]{2,1,0:T(8,128)(2,1)S(1)}, u32[]{:S(2)}) copy-start(bf16[4,64,512]{2,1,0:T(8,128)(2,1)S(1)} %collective-permute-done.5.refs_2_) | copy-start | bytes 786436
  34.8 9.7 %collective-permute-start.32 = (bf16[256,512]{1,0:T(8,128)(2,1)S(1)}, bf16[256,512]{1,0:T(8,128)(2,1)S(1)}, u32[]{:S(2)}, u32[]{:S(2)}) collective-permute-start(bf16[256,512]{1,0:T(8,128)(2,1)S(1)} %collective-permute-done.24.refs_8_), channel_id=1, source_target_pairs={{0,6},{1,7},{2,0},{3,1},{4,2},{5,3},{6,4},{7,5},{8,14},{9,15},{10,... | collective-permute-start | bytes 786440 | tf_op jit(solution)/shard_map/ppermute | solution.py:56
  37.0 19.7 %copy-start.34 = (bf16[4096,2]{0,1:T(2,128)(2,1)S(1)}, bf16[4096,2]{0,1:T(2,128)(2,1)}, u32[]{:S(2)}) copy-start(bf16[4096,2]{0,1:T(2,128)(2,1)} %param.19) | copy-start | bytes 49156
  39.8 7.2 %collective-permute-start.23 = (bf16[256,512]{1,0:T(8,128)(2,1)S(1)}, bf16[256,512]{1,0:T(8,128)(2,1)S(1)}, u32[]{:S(2)}, u32[]{:S(2)}) collective-permute-start(bf16[256,512]{1,0:T(8,128)(2,1)S(1)} %collective-permute-done.22.refs_6_), channel_id=1, source_target_pairs={{0,1},{1,0},{2,3},{3,2},{4,5},{5,4},{6,7},{7,6},{8,9},{9,8},{10,11... | collective-permute-start | bytes 786440 | tf_op jit(solution)/shard_map/ppermute | solution.py:60
  40.6 9.4 %collective-permute-start.25 = (bf16[256,512]{1,0:T(8,128)(2,1)S(1)}, bf16[256,512]{1,0:T(8,128)(2,1)S(1)}, u32[]{:S(2)}, u32[]{:S(2)}) collective-permute-start(bf16[256,512]{1,0:T(8,128)(2,1)S(1)} %collective-permute-done.24.refs_8_), channel_id=1, source_target_pairs={{0,1},{1,0},{2,3},{3,2},{4,5},{5,4},{6,7},{7,6},{8,9},{9,8},{10,11... | collective-permute-start | bytes 786440 | tf_op jit(solution)/shard_map/ppermute | solution.py:60
  41.8 9.1 %collective-permute-start.27 = (bf16[256,512]{1,0:T(8,128)(2,1)S(1)}, bf16[256,512]{1,0:T(8,128)(2,1)S(1)}, u32[]{:S(2)}, u32[]{:S(2)}) collective-permute-start(bf16[256,512]{1,0:T(8,128)(2,1)S(1)} %collective-permute-done.26.refs_10_), channel_id=1, source_target_pairs={{0,1},{1,0},{2,3},{3,2},{4,5},{5,4},{6,7},{7,6},{8,9},{9,8},{10,11... | collective-permute-start | bytes 786440 | tf_op jit(solution)/shard_map/ppermute | solution.py:60
  41.9 14.1 %copy-start.18 = (bf16[256,512]{1,0:T(8,128)(2,1)}, bf16[256,512]{1,0:T(8,128)(2,1)S(1)}, u32[]{:S(2)}) copy-start(bf16[256,512]{1,0:T(8,128)(2,1)S(1)} %collective-permute-done.30.refs_14_) | copy-start | bytes 786436
  41.9 13.4 %collective-permute-start.29 = (bf16[256,512]{1,0:T(8,128)(2,1)S(1)}, bf16[256,512]{1,0:T(8,128)(2,1)S(1)}, u32[]{:S(2)}, u32[]{:S(2)}) collective-permute-start(bf16[256,512]{1,0:T(8,128)(2,1)S(1)} %collective-permute-done.28.refs_12_), channel_id=1, source_target_pairs={{0,1},{1,0},{2,3},{3,2},{4,5},{5,4},{6,7},{7,6},{8,9},{9,8},{10,11... | collective-permute-start | bytes 786440 | tf_op jit(solution)/shard_map/ppermute | solution.py:60
  44.5 12.2 %copy-start.20 = (bf16[256,512]{1,0:T(8,128)(2,1)}, bf16[256,512]{1,0:T(8,128)(2,1)S(1)}, u32[]{:S(2)}) copy-start(bf16[256,512]{1,0:T(8,128)(2,1)S(1)} %collective-permute-done.32.refs_16_) | copy-start | bytes 786436
  44.5 12.2 %collective-permute-start.8 = (bf16[256,512]{1,0:T(8,128)(2,1)}, bf16[256,512]{1,0:T(8,128)(2,1)S(1)}, u32[]{:S(2)}, u32[]{:S(2)}) collective-permute-start(bf16[256,512]{1,0:T(8,128)(2,1)} %bitcast.10), channel_id=1, source_target_pairs={{0,2},{1,3},{2,4},{3,5},{4,6},{5,7},{6,0},{7,1},{8,10},{9,11},{10,... | collective-permute-start | bytes 786440 | tf_op jit(solution)/shard_map/ppermute | solution.py:56
  47.8 14.5 %collective-permute-start.10 = (bf16[256,512]{1,0:T(8,128)(2,1)}, bf16[256,512]{1,0:T(8,128)(2,1)S(1)}, u32[]{:S(2)}, u32[]{:S(2)}) collective-permute-start(bf16[256,512]{1,0:T(8,128)(2,1)} %bitcast.14), channel_id=1, source_target_pairs={{0,6},{1,7},{2,0},{3,1},{4,2},{5,3},{6,4},{7,5},{8,14},{9,15},{10,... | collective-permute-start | bytes 786440 | tf_op jit(solution)/shard_map/ppermute | solution.py:56
  50.7 17.2 %collective-permute-start.12 = (bf16[256,512]{1,0:T(8,128)(2,1)}, bf16[256,512]{1,0:T(8,128)(2,1)S(1)}, u32[]{:S(2)}, u32[]{:S(2)}) collective-permute-start(bf16[256,512]{1,0:T(8,128)(2,1)} %bitcast.15), channel_id=1, source_target_pairs={{0,2},{1,3},{2,4},{3,5},{4,6},{5,7},{6,0},{7,1},{8,10},{9,11},{10,... | collective-permute-start | bytes 786440 | tf_op jit(solution)/shard_map/ppermute | solution.py:56
  51.6 21.7 %collective-permute-start.14 = (bf16[256,512]{1,0:T(8,128)(2,1)}, bf16[256,512]{1,0:T(8,128)(2,1)S(1)}, u32[]{:S(2)}, u32[]{:S(2)}) collective-permute-start(bf16[256,512]{1,0:T(8,128)(2,1)} %bitcast.11), channel_id=1, source_target_pairs={{0,6},{1,7},{2,0},{3,1},{4,2},{5,3},{6,4},{7,5},{8,14},{9,15},{10,... | collective-permute-start | bytes 786440 | tf_op jit(solution)/shard_map/ppermute | solution.py:56
  55.3 0.7 copy-start.28
  56.0 19.1 %collective-permute-start.6 = (bf16[256,512]{1,0:T(8,128)(2,1)}, bf16[256,512]{1,0:T(8,128)(2,1)S(1)}, u32[]{:S(2)}, u32[]{:S(2)}) collective-permute-start(bf16[256,512]{1,0:T(8,128)(2,1)} %bitcast.12), channel_id=1, source_target_pairs={{0,1},{1,0},{2,3},{3,2},{4,5},{5,4},{6,7},{7,6},{8,9},{9,8},{10,11... | collective-permute-start | bytes 786440 | tf_op jit(solution)/shard_map/ppermute | solution.py:60
  56.7 18.6 %collective-permute-start.7 = (bf16[256,512]{1,0:T(8,128)(2,1)}, bf16[256,512]{1,0:T(8,128)(2,1)S(1)}, u32[]{:S(2)}, u32[]{:S(2)}) collective-permute-start(bf16[256,512]{1,0:T(8,128)(2,1)} %bitcast.16), channel_id=1, source_target_pairs={{0,1},{1,0},{2,3},{3,2},{4,5},{5,4},{6,7},{7,6},{8,9},{9,8},{10,11... | collective-permute-start | bytes 786440 | tf_op jit(solution)/shard_map/ppermute | solution.py:60
  58.1 31.0 %copy-start.30 = (f32[2]{0:T(128)S(1)}, f32[2]{0:T(128)}, u32[]{:S(2)}) copy-start(f32[2]{0:T(128)} %refs_1_.1) | copy-start | bytes 28
  59.7 29.4 %copy-start.5 = (bf16[4096,256]{1,0:T(8,128)(2,1)S(1)}, bf16[4096,256]{1,0:T(8,128)(2,1)}, u32[]{:S(2)}) copy-start(bf16[4096,256]{1,0:T(8,128)(2,1)} %refs_18_.2) | copy-start | bytes 6291460
  62.3 14.3 %collective-permute-start.31 = (bf16[256,512]{1,0:T(8,128)(2,1)}, bf16[256,512]{1,0:T(8,128)(2,1)S(1)}, u32[]{:S(2)}, u32[]{:S(2)}) collective-permute-start(bf16[256,512]{1,0:T(8,128)(2,1)} %copy-done.18), channel_id=1, source_target_pairs={{0,1},{1,0},{2,3},{3,2},{4,5},{5,4},{6,7},{7,6},{8,9},{9,8},{10,11... | collective-permute-start | bytes 786440 | tf_op jit(solution)/shard_map/ppermute | solution.py:60
  68.0 8.9 %collective-permute-start.33 = (bf16[256,512]{1,0:T(8,128)(2,1)}, bf16[256,512]{1,0:T(8,128)(2,1)S(1)}, u32[]{:S(2)}, u32[]{:S(2)}) collective-permute-start(bf16[256,512]{1,0:T(8,128)(2,1)} %copy-done.20), channel_id=1, source_target_pairs={{0,1},{1,0},{2,3},{3,2},{4,5},{5,4},{6,7},{7,6},{8,9},{9,8},{10,11... | collective-permute-start | bytes 786440 | tf_op jit(solution)/shard_map/ppermute | solution.py:60
  73.3 15.2 %collective-permute-start.18 = (bf16[256,512]{1,0:T(8,128)(2,1)S(1)}, bf16[256,512]{1,0:T(8,128)(2,1)S(1)}, u32[]{:S(2)}, u32[]{:S(2)}) collective-permute-start(bf16[256,512]{1,0:T(8,128)(2,1)S(1)} %collective-permute-done.10.refs_7_), channel_id=1, source_target_pairs={{0,6},{1,7},{2,0},{3,1},{4,2},{5,3},{6,4},{7,5},{8,14},{9,15},{10,... | collective-permute-start | bytes 786440 | tf_op jit(solution)/shard_map/ppermute | solution.py:56
  75.0 14.0 %collective-permute-start.11 = (bf16[256,512]{1,0:T(8,128)(2,1)S(1)}, bf16[256,512]{1,0:T(8,128)(2,1)S(1)}, u32[]{:S(2)}, u32[]{:S(2)}) collective-permute-start(bf16[256,512]{1,0:T(8,128)(2,1)S(1)} %collective-permute-done.10.refs_7_), channel_id=1, source_target_pairs={{0,1},{1,0},{2,3},{3,2},{4,5},{5,4},{6,7},{7,6},{8,9},{9,8},{10,11... | collective-permute-start | bytes 786440 | tf_op jit(solution)/shard_map/ppermute | solution.py:60
  75.3 13.2 %collective-permute-start.16 = (bf16[256,512]{1,0:T(8,128)(2,1)S(1)}, bf16[256,512]{1,0:T(8,128)(2,1)S(1)}, u32[]{:S(2)}, u32[]{:S(2)}) collective-permute-start(bf16[256,512]{1,0:T(8,128)(2,1)S(1)} %collective-permute-done.8.refs_5_), channel_id=1, source_target_pairs={{0,2},{1,3},{2,4},{3,5},{4,6},{5,7},{6,0},{7,1},{8,10},{9,11},{10,... | collective-permute-start | bytes 786440 | tf_op jit(solution)/shard_map/ppermute | solution.py:56
  76.6 38.1 %collective-permute-start.9 = (bf16[256,512]{1,0:T(8,128)(2,1)S(1)}, bf16[256,512]{1,0:T(8,128)(2,1)S(1)}, u32[]{:S(2)}, u32[]{:S(2)}) collective-permute-start(bf16[256,512]{1,0:T(8,128)(2,1)S(1)} %collective-permute-done.8.refs_5_), channel_id=1, source_target_pairs={{0,1},{1,0},{2,3},{3,2},{4,5},{5,4},{6,7},{7,6},{8,9},{9,8},{10,11... | collective-permute-start | bytes 786440 | tf_op jit(solution)/shard_map/ppermute | solution.py:60
  76.8 37.8 %collective-permute-start.13 = (bf16[256,512]{1,0:T(8,128)(2,1)S(1)}, bf16[256,512]{1,0:T(8,128)(2,1)S(1)}, u32[]{:S(2)}, u32[]{:S(2)}) collective-permute-start(bf16[256,512]{1,0:T(8,128)(2,1)S(1)} %collective-permute-done.12.refs_9_), channel_id=1, source_target_pairs={{0,1},{1,0},{2,3},{3,2},{4,5},{5,4},{6,7},{7,6},{8,9},{9,8},{10,11... | collective-permute-start | bytes 786440 | tf_op jit(solution)/shard_map/ppermute | solution.py:60
  88.5 26.2 %collective-permute-start.15 = (bf16[256,512]{1,0:T(8,128)(2,1)S(1)}, bf16[256,512]{1,0:T(8,128)(2,1)S(1)}, u32[]{:S(2)}, u32[]{:S(2)}) collective-permute-start(bf16[256,512]{1,0:T(8,128)(2,1)S(1)} %collective-permute-done.14.refs_11_), channel_id=1, source_target_pairs={{0,1},{1,0},{2,3},{3,2},{4,5},{5,4},{6,7},{7,6},{8,9},{9,8},{10,11... | collective-permute-start | bytes 786440 | tf_op jit(solution)/shard_map/ppermute | solution.py:60
  88.5 26.2 %collective-permute-start.17 = (bf16[256,512]{1,0:T(8,128)(2,1)S(1)}, bf16[256,512]{1,0:T(8,128)(2,1)S(1)}, u32[]{:S(2)}, u32[]{:S(2)}) collective-permute-start(bf16[256,512]{1,0:T(8,128)(2,1)S(1)} %collective-permute-done.16.refs_13_), channel_id=1, source_target_pairs={{0,1},{1,0},{2,3},{3,2},{4,5},{5,4},{6,7},{7,6},{8,9},{9,8},{10,11... | collective-permute-start | bytes 786440 | tf_op jit(solution)/shard_map/ppermute | solution.py:60
  89.0 25.7 %collective-permute-start.19 = (bf16[256,512]{1,0:T(8,128)(2,1)S(1)}, bf16[256,512]{1,0:T(8,128)(2,1)S(1)}, u32[]{:S(2)}, u32[]{:S(2)}) collective-permute-start(bf16[256,512]{1,0:T(8,128)(2,1)S(1)} %collective-permute-done.18.refs_15_), channel_id=1, source_target_pairs={{0,1},{1,0},{2,3},{3,2},{4,5},{5,4},{6,7},{7,6},{8,9},{9,8},{10,11... | collective-permute-start | bytes 786440 | tf_op jit(solution)/shard_map/ppermute | solution.py:60
  89.1 1.6 %copy-start.6 = (bf16[4096,256]{1,0:T(8,128)(2,1)S(1)}, bf16[4096,256]{1,0:T(8,128)(2,1)}, u32[]{:S(2)}) copy-start(bf16[4096,256]{1,0:T(8,128)(2,1)} %refs_19_.1) | copy-start | bytes 6291460
  90.7 1.6 %copy-start.7 = (bf16[4096,256]{1,0:T(8,128)(2,1)S(1)}, bf16[4096,256]{1,0:T(8,128)(2,1)}, u32[]{:S(2)}) copy-start(bf16[4096,256]{1,0:T(8,128)(2,1)} %refs_21_.1) | copy-start | bytes 6291460
  92.3 0.9 copy-start.9
  93.2 0.9 copy-start.11
  94.2 0.9 copy-start.13
  95.1 0.9 copy-start.15
  96.1 0.9 copy-start.17
  97.0 0.9 copy-start.19
  98.0 0.9 copy-start.21
  98.9 0.9 copy-start.23
  99.9 0.9 copy-start.25
  100.8 0.9 copy-start.27
  101.8 0.9 copy-start.29
  102.7 12.0 %copy-start = (bf16[4096,256]{1,0:T(8,128)(2,1)S(1)}, bf16[4096,256]{1,0:T(8,128)(2,1)}, u32[]{:S(2)}) copy-start(bf16[4096,256]{1,0:T(8,128)(2,1)} %refs_17_.1) | copy-start | bytes 6291460
  102.7 12.0 %copy-start.1 = (bf16[4096,256]{1,0:T(8,128)(2,1)S(1)}, bf16[4096,256]{1,0:T(8,128)(2,1)}, u32[]{:S(2)}) copy-start(bf16[4096,256]{1,0:T(8,128)(2,1)} %refs_18_.3) | copy-start | bytes 6291460
  102.7 12.0 %copy-start.2 = (bf16[4,64,512]{2,1,0:T(8,128)(2,1)S(1)}, bf16[4,64,512]{2,1,0:T(8,128)(2,1)}, u32[]{:S(2)}) copy-start(bf16[4,64,512]{2,1,0:T(8,128)(2,1)} %get-tuple-element.16) | copy-start | bytes 786436
  102.7 12.0 %copy-start.3 = (bf16[4,64,512]{2,1,0:T(8,128)(2,1)S(1)}, bf16[4,64,512]{2,1,0:T(8,128)(2,1)}, u32[]{:S(2)}) copy-start(bf16[4,64,512]{2,1,0:T(8,128)(2,1)} %get-tuple-element.17) | copy-start | bytes 786436
  102.7 12.0 %copy-start.4 = (bf16[2,128,256]{2,1,0:T(8,128)(2,1)S(1)}, bf16[2,128,256]{2,1,0:T(8,128)(2,1)}, u32[]{:S(2)}) copy-start(bf16[2,128,256]{2,1,0:T(8,128)(2,1)} %refs_22_.1) | copy-start | bytes 393220
  (6 other events, 4.2 us)
where the time goes:
time: 122 us; the launch traced here: 121 us
  waiting for transfers between devices  35.7 us (29%)
  starting transfers between devices  35.1 us (29%)
  Pallas kernels  23.9 us (20%)
  local copies, waits for them, and re-layouts  23.5 us (19%)
  other arithmetic  2.61 us (2%)
    ppermute x12, waiting for transfers between devices, step(): return lax.ppermute(value, 'tp', moves)  28.5 us
    ppermute x12, starting transfers between devices, step(): return lax.ppermute(value, 'tp', moves)  21.2 us
    unnamed x74, local copies, waits for them, and re-layouts  20.8 us
    pallas_call x1, Pallas kernels, project(): pl.pallas_call(functools.partial(project_kernel, places, heads), out_shap...  11.9 us
    ppermute x6, starting transfers between devices, exchange(): return lax.ppermute(value, 'st', [(i, i ^ k) for i in range(group_count)])  11 us
    ppermute x6, waiting for transfers between devices, exchange(): return lax.ppermute(value, 'st', [(i, i ^ k) for i in range(group_count)])  7.17 us
    pallas_call x1, Pallas kernels, passages(): pl.pallas_call(functools.partial(passage_kernel, places, heads, picks), o...  6.5 us
    ppermute x16, starting transfers between devices, swap(): return lax.ppermute(value, 'tp', moves)  2.95 us
  transfers between devices with their start and end apart: 34, of which 10 were waited for; matrix products, arithmetic and copies ran while one was open for 5% of the time, Pallas kernels for 14%

commit v1 on v0

--- a/solution.py
+++ b/solution.py
@@ -27,6 +27,7 @@
 ANY = pl.BlockSpec(memory_space=pl.ANY)
 SMEM = pl.BlockSpec(memory_space=pltpu.SMEM)
 VMEM = pl.BlockSpec(memory_space=pltpu.VMEM)
+HBM = pl.BlockSpec(memory_space=pltpu.HBM)
 
 
 def rotary_tables(rows):
@@ -190,7 +191,7 @@
             jax.ShapeDtypeStruct((rows, heads * MEM_DIM), bf16),
             jax.ShapeDtypeStruct((rows, LANES), f32),
         ),
-        in_specs=[SMEM, SMEM] + [ANY] * (len(parts) + len(weights)) + [VMEM, VMEM],
+        in_specs=[SMEM, SMEM] + [ANY] * len(parts) + [HBM] * len(weights) + [VMEM, VMEM],
         out_specs=(VMEM, VMEM, VMEM),
         scratch_shapes=[
             pltpu.VMEM((slots, rows, depth), bf16),
@@ -263,23 +264,19 @@
     )(source, index, store, *arrived)
 
 
-def passage_kernel(places, heads, picks, *refs):
-    count = len(places)
-    order = refs[0]
-    parts = refs[1 : 1 + count]
-    weights = refs[1 + count : 3 + count]
-    query, gate, norm, lift, out, xs, ws, acc, sem_x, sem_w = refs[3 + count :]
+def sum_slots(places, start, order, parts, weights, acc, xs, ws, sem_x, sem_w):
     slots = ws.shape[0]
     depth = ws.shape[1]
-    width = heads * MEM_DIM
+    width = weights[0].shape[1]
     copies = [[] for _ in range(slots)]
     for p, (slot, first) in enumerate(places):
         extent = parts[p].shape[0]
-        copies[slot].append(
-            pltpu.make_async_copy(parts[p], xs.at[slot, pl.ds(first, extent)], sem_x.at[p])
+        at = slot - start
+        copies[at].append(
+            pltpu.make_async_copy(parts[p], xs.at[at, pl.ds(first, extent)], sem_x.at[p])
         )
     for slot in range(slots):
-        row = pl.multiple_of(order[slot] * depth, depth)
+        row = pl.multiple_of(order[slot + start] * depth, depth)
         for w, weight in enumerate(weights):
             copies[slot].append(
                 pltpu.make_async_copy(
@@ -294,10 +291,57 @@
     for slot in range(slots):
         for copy in copies[slot]:
             copy.wait()
-        if slot == 0:
-            acc[...] = dot(xs[slot], ws[slot])
-        else:
-            acc[...] += dot(xs[slot], ws[slot])
+        acc[...] += dot(xs[slot], ws[slot])
+
+
+def near_kernel(places, *refs):
+    count = len(places)
+    order = refs[0]
+    parts = refs[1 : 1 + count]
+    weights = refs[1 + count : 3 + count]
+    acc, xs, ws, sem_x, sem_w = refs[3 + count :]
+    acc[...] = jnp.zeros_like(acc)
+    sum_slots(places, 0, order, parts, weights, acc, xs, ws, sem_x, sem_w)
+
+
+def slot_scratch(parts, weights, slots):
+    rows, depth = 2 * parts[0][0].shape[0], parts[0][0].shape[1]
+    width = sum(w.shape[1] for w in weights)
+    return [
+        pltpu.VMEM((slots, rows, depth), bf16),
+        pltpu.VMEM((slots, depth, width), bf16),
+        pltpu.SemaphoreType.DMA((len(parts),)),
+        pltpu.SemaphoreType.DMA((slots, len(weights))),
+    ]
+
+
+def near_passages(parts, order, weights, slots):
+    places = tuple((slot, first) for _, slot, first in parts)
+    rows, depth = 2 * parts[0][0].shape[0], parts[0][0].shape[1]
+    width = sum(w.shape[1] for w in weights)
+    return pl.pallas_call(
+        functools.partial(near_kernel, places),
+        out_shape=jax.ShapeDtypeStruct((rows, width), f32),
+        in_specs=[SMEM] + [ANY] * len(parts) + [HBM] * len(weights),
+        out_specs=VMEM,
+        scratch_shapes=slot_scratch(parts, weights, slots),
+        compiler_params=pltpu.CompilerParams(vmem_limit_bytes=24 * 1024 * 1024),
+        cost_estimate=pl.CostEstimate(
+            flops=2 * rows * depth * slots * width, bytes_accessed=0, transcendentals=0
+        ),
+        name="passage_near",
+    )(order, *[p[0] for p in parts], *weights)
+
+
+def passage_kernel(places, start, heads, picks, *refs):
+    count = len(places)
+    order = refs[0]
+    parts = refs[1 : 1 + count]
+    weights = refs[1 + count : 3 + count]
+    near, query, gate, norm, lift, out, acc, xs, ws, sem_x, sem_w = refs[3 + count :]
+    width = heads * MEM_DIM
+    acc[...] = near[...]
+    sum_slots(places, start, order, parts, weights, acc, xs, ws, sem_x, sem_w)
     block_rows = picks * PASS_ROWS
     for h in range(heads):
         lo, hi = h * MEM_DIM, (h + 1) * MEM_DIM
@@ -323,30 +367,24 @@
             ).astype(bf16)
 
 
-def passages(parts, order, weights, query, gate, norm, lift, picks):
+def passages(parts, order, weights, near, query, gate, norm, lift, picks, start):
     heads = lift.shape[0]
     places = tuple((slot, first) for _, slot, first in parts)
     rows, depth = 2 * parts[0][0].shape[0], parts[0][0].shape[1]
-    slots = order.shape[0]
+    slots = order.shape[0] - start
     width = sum(w.shape[1] for w in weights)
     return pl.pallas_call(
-        functools.partial(passage_kernel, places, heads, picks),
+        functools.partial(passage_kernel, places, start, heads, picks),
         out_shape=jax.ShapeDtypeStruct(norm.shape, bf16),
-        in_specs=[SMEM] + [ANY] * (len(parts) + len(weights)) + [VMEM] * 4,
+        in_specs=[SMEM] + [ANY] * len(parts) + [HBM] * len(weights) + [VMEM] * 5,
         out_specs=VMEM,
-        scratch_shapes=[
-            pltpu.VMEM((slots, rows, depth), bf16),
-            pltpu.VMEM((slots, depth, width), bf16),
-            pltpu.VMEM((rows, width), f32),
-            pltpu.SemaphoreType.DMA((len(parts),)),
-            pltpu.SemaphoreType.DMA((slots, len(weights))),
-        ],
-        compiler_params=pltpu.CompilerParams(vmem_limit_bytes=32 * 1024 * 1024),
+        scratch_shapes=[pltpu.VMEM((rows, width), f32)] + slot_scratch(parts, weights, slots),
+        compiler_params=pltpu.CompilerParams(vmem_limit_bytes=24 * 1024 * 1024),
         cost_estimate=pl.CostEstimate(
             flops=2 * rows * depth * slots * width, bytes_accessed=0, transcendentals=0
         ),
         name="passage_mix",
-    )(order, *[p[0] for p in parts], *weights, query, gate, norm, lift)
+    )(order, *[p[0] for p in parts], *weights, near, query, gate, norm, lift)
 
 
 def per_device(
@@ -375,6 +413,9 @@
     def exchange(value, k):
         return lax.ppermute(value, "st", [(i, i ^ k) for i in range(group_count)])
 
+    def exchange_all(values):
+        return [exchange(value, k + 1) for k, value in enumerate(values)]
+
     wanted = passage_ids.reshape(request_count)
     owners = wanted // held_count
     held_index = wanted % held_count
@@ -387,14 +428,14 @@
         place[:, None] == jnp.arange(group_count * capacity, dtype=jnp.int32)[None, :]
     ).astype(jnp.int32)
     outgoing = jnp.sum(selector * held_index[:, None], axis=0).reshape(group_count, capacity)
-    incoming = [exchange(outgoing[k], k) for k in range(1, group_count)]
+    incoming = exchange_all([outgoing[k] for k in range(1, group_count)])
 
     half = tokens.shape[0] // 2
     token_halves = (tokens[:half], tokens[half:])
     token_parts, order = ring_gather(token_halves, ring_size, core_count)
 
     fetched = fetch(store, jnp.concatenate(incoming), group_count - 1)
-    arrived = [exchange(fetched[k - 1], k) for k in range(1, group_count)]
+    arrived = exchange_all(fetched)
     rows_at = jnp.where(source == 0, held_index, slot_index)
     own_rows = compact(store, arrived, source, rows_at)
     own_rows = [x.reshape(-1, store.shape[2]) for x in own_rows]
@@ -409,8 +450,12 @@
         decay_rate,
         tables,
     )
+    start = order.shape[0] - core_count
+    mem_weights = (w_mem_key, w_mem_value)
+    near = near_passages([p for p in row_parts if p[1] < start], order, mem_weights, start)
+    far = [p for p in row_parts if p[1] >= start]
     return passages(
-        row_parts, order, (w_mem_key, w_mem_value), query, gate, norm, w_lift, picks
+        far, order, mem_weights, near, query, gate, norm, w_lift, picks, start
     )
 
 

time: 122 us -> 122 us (level)
  waiting for transfers between devices: 35.7 us -> 33.2 us
  starting transfers between devices: 35.1 us -> 37 us
    ppermute x12, waiting for transfers between devices: 28.5 us -> 26 us  [step(): return lax.ppermute(value, 'tp', moves)]
    ppermute x12, starting transfers between devices: 21.2 us -> 23.2 us  [step(): return lax.ppermute(value, 'tp', moves)]
    pallas_call x1 -> x2, Pallas kernels: 6.5 us -> 7.3 us  [the longest x1 3.94 us: passages(): pl.pallas_call(functools.partial(passage_kernel, places, start, heads, pi...]
  transfers between devices with their start and end apart: 34 -> 34, of which waited for: 10 -> 10; matrix products, arithmetic and copies ran while one was open for 5% -> 5% of each run, Pallas kernels for 14% -> 17%
where the time goes in v1:
time: 122 us
  starting transfers between devices  37 us (30%)
  waiting for transfers between devices  33.2 us (27%)
  Pallas kernels  24.7 us (20%)
  local copies, waits for them, and re-layouts  23.5 us (19%)
  other arithmetic  2.61 us (2%)
    ppermute x12, waiting for transfers between devices, step(): return lax.ppermute(value, 'tp', moves)  26 us
    ppermute x12, starting transfers between devices, step(): return lax.ppermute(value, 'tp', moves)  23.2 us
    unnamed x74, local copies, waits for them, and re-layouts  20.8 us
    pallas_call x1, Pallas kernels, project(): pl.pallas_call(functools.partial(project_kernel, places, heads), out_shap...  11.9 us
    ppermute x6, starting transfers between devices, exchange(): return lax.ppermute(value, 'st', [(i, i ^ k) for i in range(group_count)])  11 us
    ppermute x6, waiting for transfers between devices, exchange(): return lax.ppermute(value, 'st', [(i, i ^ k) for i in range(group_count)])  7.17 us
    pallas_call x1, Pallas kernels, passages(): pl.pallas_call(functools.partial(passage_kernel, places, start, heads, pi...  3.94 us
    pallas_call x1, Pallas kernels, near_passages(): pl.pallas_call(functools.partial(near_kernel, places), out_shape=jax.Shap...  3.36 us
  transfers between devices with their start and end apart: 34, of which 10 were waited for; matrix products, arithmetic and copies ran while one was open for 5% of the time, Pallas kernels for 17%

profile of v1, /device:TPU:0, one launch (start us, length us, event | category | flops | bytes accessed | tf_op | source)
XLA Modules:
  0.0 121.6 jit_solution(12681392950211071092)
XLA Ops:
  0.0 1.1 fusion.6
  1.1 5.1 %collective-permute-start.24 = (bf16[256,512]{1,0:T(8,128)(2,1)S(1)}, bf16[256,512]{1,0:T(8,128)(2,1)S(1)}, u32[]{:S(2)}, u32[]{:S(2)}) collective-permute-start(bf16[256,512]{1,0:T(8,128)(2,1)S(1)} %get-tuple-element.25.refs_4_), channel_id=1, source_target_pairs={{0,6},{1,7},{2,0},{3,1},{4,2},{5,3},{6,4},{7,5},{8,14},{9,15},{10,... | collective-permute-start | bytes 786440 | tf_op jit(solution)/shard_map/ppermute | solution.py:57
  6.2 0.8 copy.17
  7.3 0.5 compare_select_fusion
  7.9 1.5 %collective-permute-start = (s32[4]{0:T(128)S(1)}, s32[4]{0:T(128)S(1)}, u32[]{:S(2)}, u32[]{:S(2)}) collective-permute-start(s32[4]{0:T(128)S(1)} %get-tuple-element.30), channel_id=1, source_target_pairs={{0,8},{8,0},{16,24},{24,16},{1,9},{9,1},{17,25},{25,17},{2,10},{10... | collective-permute-start | bytes 56 | tf_op jit(solution)/shard_map/ppermute | solution.py:414
  9.4 1.5 %collective-permute-start.1 = (s32[4]{0:T(128)S(1)}, s32[4]{0:T(128)S(1)}, u32[]{:S(2)}, u32[]{:S(2)}) collective-permute-start(s32[4]{0:T(128)S(1)} %get-tuple-element.32), channel_id=1, source_target_pairs={{0,16},{8,24},{16,0},{24,8},{1,17},{9,25},{17,1},{25,9},{2,18},{10... | collective-permute-start | bytes 56 | tf_op jit(solution)/shard_map/ppermute | solution.py:414
  10.9 0.6 collective-permute-done
  11.5 2.4 %collective-permute-start.2 = (s32[4]{0:T(128)S(1)}, s32[4]{0:T(128)S(1)}, u32[]{:S(2)}, u32[]{:S(2)}) collective-permute-start(s32[4]{0:T(128)S(1)} %get-tuple-element.31), channel_id=1, source_target_pairs={{0,24},{8,16},{16,8},{24,0},{1,25},{9,17},{17,9},{25,1},{2,26},{10... | collective-permute-start | bytes 56 | tf_op jit(solution)/shard_map/ppermute | solution.py:414
  14.0 2.0 %collective-permute-done.2 = s32[4]{0:T(128)S(1)} collective-permute-done((s32[4]{0:T(128)S(1)}, s32[4]{0:T(128)S(1)}, u32[]{:S(2)}, u32[]{:S(2)}) %collective-permute-start.2) | collective-permute-done | bytes 48 | tf_op jit(solution)/shard_map/ppermute | solution.py:414
  16.0 0.6 pad_add_fusion.index
  16.6 2.8 %fetch_rows.1 = (bf16[4,64,512]{2,1,0:T(8,128)(2,1)}, bf16[4,64,512]{2,1,0:T(8,128)(2,1)}, bf16[4,64,512]{2,1,0:T(8,128)(2,1)}) custom-call(s32[12]{0:T(128)} %pad_add_fusion.index, bf16[128,64,512]{2,1,0:T(8,128)(2,1)} %store.3), custom_call_target="tpu_custom_call" | custom-call | tf_op jit(solution)/shard_map/fetch_rows/pallas_call | solution.py:227
  19.4 1.6 %collective-permute-start.3 = (bf16[4,64,512]{2,1,0:T(8,128)(2,1)}, bf16[4,64,512]{2,1,0:T(8,128)(2,1)S(1)}, u32[]{:S(2)}, u32[]{:S(2)}) collective-permute-start(bf16[4,64,512]{2,1,0:T(8,128)(2,1)} %get-tuple-element.13), channel_id=1, source_target_pairs={{0,8},{8,0},{16,24},{24,16},{1,9},{9,1},{17,25},{25,17},{2,10},{10... | collective-permute-start | bytes 786440 | tf_op jit(solution)/shard_map/ppermute | solution.py:414
  21.0 1.5 %collective-permute-start.4 = (bf16[4,64,512]{2,1,0:T(8,128)(2,1)}, bf16[4,64,512]{2,1,0:T(8,128)(2,1)S(1)}, u32[]{:S(2)}, u32[]{:S(2)}) collective-permute-start(bf16[4,64,512]{2,1,0:T(8,128)(2,1)} %get-tuple-element.14), channel_id=1, source_target_pairs={{0,16},{8,24},{16,0},{24,8},{1,17},{9,25},{17,1},{25,9},{2,18},{10... | collective-permute-start | bytes 786440 | tf_op jit(solution)/shard_map/ppermute | solution.py:414
  22.5 1.4 %collective-permute-done.22.refs_6_ = bf16[256,512]{1,0:T(8,128)(2,1)S(1)} collective-permute-done((bf16[256,512]{1,0:T(8,128)(2,1)S(1)}, bf16[256,512]{1,0:T(8,128)(2,1)S(1)}, u32[]{:S(2)}, u32[]{:S(2)}) %collective-permute-start.22) | collective-permute-done | bytes 262176 | tf_op jit(solution)/shard_map/ppermute | solution.py:57
  23.9 2.4 %collective-permute-start.5 = (bf16[4,64,512]{2,1,0:T(8,128)(2,1)}, bf16[4,64,512]{2,1,0:T(8,128)(2,1)S(1)}, u32[]{:S(2)}, u32[]{:S(2)}) collective-permute-start(bf16[4,64,512]{2,1,0:T(8,128)(2,1)} %get-tuple-element.15), channel_id=1, source_target_pairs={{0,24},{8,16},{16,8},{24,0},{1,25},{9,17},{17,9},{25,1},{2,26},{10... | collective-permute-start | bytes 786440 | tf_op jit(solution)/shard_map/ppermute | solution.py:414
  26.4 1.7 %collective-permute-start.28 = (bf16[256,512]{1,0:T(8,128)(2,1)S(1)}, bf16[256,512]{1,0:T(8,128)(2,1)S(1)}, u32[]{:S(2)}, u32[]{:S(2)}) collective-permute-start(bf16[256,512]{1,0:T(8,128)(2,1)S(1)} %get-tuple-element.26.refs_2_), channel_id=1, source_target_pairs={{0,6},{1,7},{2,0},{3,1},{4,2},{5,3},{6,4},{7,5},{8,14},{9,15},{10,... | collective-permute-start | bytes 786440 | tf_op jit(solution)/shard_map/ppermute | solution.py:57
  28.1 0.5 collective-permute-start.21
  28.6 4.6 %collective-permute-done.4.refs_1_ = bf16[4,64,512]{2,1,0:T(8,128)(2,1)S(1)} collective-permute-done((bf16[4,64,512]{2,1,0:T(8,128)(2,1)}, bf16[4,64,512]{2,1,0:T(8,128)(2,1)S(1)}, u32[]{:S(2)}, u32[]{:S(2)}) %collective-permute-start.4) | collective-permute-done | bytes 262176 | tf_op jit(solution)/shard_map/ppermute | solution.py:414
  33.2 1.6 %collective-permute-start.30 = (bf16[256,512]{1,0:T(8,128)(2,1)S(1)}, bf16[256,512]{1,0:T(8,128)(2,1)S(1)}, u32[]{:S(2)}, u32[]{:S(2)}) collective-permute-start(bf16[256,512]{1,0:T(8,128)(2,1)S(1)} %collective-permute-done.22.refs_6_), channel_id=1, source_target_pairs={{0,2},{1,3},{2,4},{3,5},{4,6},{5,7},{6,0},{7,1},{8,10},{9,11},{10,... | collective-permute-start | bytes 786440 | tf_op jit(solution)/shard_map/ppermute | solution.py:57
  34.8 2.3 %collective-permute-start.32 = (bf16[256,512]{1,0:T(8,128)(2,1)S(1)}, bf16[256,512]{1,0:T(8,128)(2,1)S(1)}, u32[]{:S(2)}, u32[]{:S(2)}) collective-permute-start(bf16[256,512]{1,0:T(8,128)(2,1)S(1)} %collective-permute-done.24.refs_8_), channel_id=1, source_target_pairs={{0,6},{1,7},{2,0},{3,1},{4,2},{5,3},{6,4},{7,5},{8,14},{9,15},{10,... | collective-permute-start | bytes 786440 | tf_op jit(solution)/shard_map/ppermute | solution.py:57
  37.1 2.8 %compact_rows.1 = (bf16[4,64,512]{2,1,0:T(8,128)(2,1)}, bf16[4,64,512]{2,1,0:T(8,128)(2,1)}) custom-call(s32[8]{0:T(128)} %copy-done.35, s32[8]{0:T(128)} %get-tuple-element.23.index, bf16[128,64,512]{2,1,0:T(8,128)(2,1)} %store.3, bf16[4,64,512]{2,1,0:T(8,128)(2,1)} %copy-done.31, bf16[4,64,512]{2,1,0:T(8,128)(2,1)} %copy-done.32, ...), custom_call_target="tpu_custom_call" | custom-call | tf_op jit(solution)/shard_map/compact_rows/pallas_call | solution.py:257
  39.9 0.7 copy-done.14
  40.6 0.5 collective-permute-start.25
  41.1 0.7 copy-done.16
  41.9 0.5 collective-permute-start.29
  42.4 0.7 copy-done.12
  43.0 1.5 %collective-permute-done.32.refs_16_ = bf16[256,512]{1,0:T(8,128)(2,1)S(1)} collective-permute-done((bf16[256,512]{1,0:T(8,128)(2,1)S(1)}, bf16[256,512]{1,0:T(8,128)(2,1)S(1)}, u32[]{:S(2)}, u32[]{:S(2)}) %collective-permute-start.32) | collective-permute-done | bytes 262176 | tf_op jit(solution)/shard_map/ppermute | solution.py:57
  44.5 2.5 %collective-permute-start.6 = (bf16[256,512]{1,0:T(8,128)(2,1)}, bf16[256,512]{1,0:T(8,128)(2,1)S(1)}, u32[]{:S(2)}, u32[]{:S(2)}) collective-permute-start(bf16[256,512]{1,0:T(8,128)(2,1)} %bitcast.10), channel_id=1, source_target_pairs={{0,2},{1,3},{2,4},{3,5},{4,6},{5,7},{6,0},{7,1},{8,10},{9,11},{10,... | collective-permute-start | bytes 786440 | tf_op jit(solution)/shard_map/ppermute | solution.py:57
  47.1 0.7 copy-done.22
  47.8 2.3 %collective-permute-start.9 = (bf16[256,512]{1,0:T(8,128)(2,1)}, bf16[256,512]{1,0:T(8,128)(2,1)S(1)}, u32[]{:S(2)}, u32[]{:S(2)}) collective-permute-start(bf16[256,512]{1,0:T(8,128)(2,1)} %bitcast.14), channel_id=1, source_target_pairs={{0,6},{1,7},{2,0},{3,1},{4,2},{5,3},{6,4},{7,5},{8,14},{9,15},{10,... | collective-permute-start | bytes 786440 | tf_op jit(solution)/shard_map/ppermute | solution.py:57
  50.0 0.7 copy-done.24
  50.7 0.2 collective-permute-start.16
  50.9 0.7 copy-done.26
  51.6 3.6 %collective-permute-start.18 = (bf16[256,512]{1,0:T(8,128)(2,1)}, bf16[256,512]{1,0:T(8,128)(2,1)S(1)}, u32[]{:S(2)}, u32[]{:S(2)}) collective-permute-start(bf16[256,512]{1,0:T(8,128)(2,1)} %bitcast.11), channel_id=1, source_target_pairs={{0,6},{1,7},{2,0},{3,1},{4,2},{5,3},{6,4},{7,5},{8,14},{9,15},{10,... | collective-permute-start | bytes 786440 | tf_op jit(solution)/shard_map/ppermute | solution.py:57
  55.3 0.7 copy-done.28
  56.0 0.7 collective-permute-done.6.refs_5_
  56.7 1.4 %copy.18 = bf16[4096,2]{1,0:T(8,128)(2,1)} copy(bf16[4096,2]{0,1:T(2,128)(2,1)S(1)} %copy-done.34) | data formatting | bytes 32768 | tf_op args[7]
  58.1 1.4 %pad.4.refs_22_ = bf16[4096,128]{1,0:T(8,128)(2,1)S(1)} pad(bf16[4096,2]{1,0:T(8,128)(2,1)} %copy.18, bf16[]{:T(256)} %constant.65.clone.1), padding=0_0x0_126 | pad | bytes 1064962 | tf_op jit(solution)/shard_map/jit(_pad)/pad | solution.py:444
  59.7 2.6 %collective-permute-done.9.refs_7_ = bf16[256,512]{1,0:T(8,128)(2,1)S(1)} collective-permute-done((bf16[256,512]{1,0:T(8,128)(2,1)}, bf16[256,512]{1,0:T(8,128)(2,1)S(1)}, u32[]{:S(2)}, u32[]{:S(2)}) %collective-permute-start.9) | collective-permute-done | bytes 262176 | tf_op jit(solution)/shard_map/ppermute | solution.py:57
  62.3 5.7 %collective-permute-done.16.refs_9_ = bf16[256,512]{1,0:T(8,128)(2,1)S(1)} collective-permute-done((bf16[256,512]{1,0:T(8,128)(2,1)}, bf16[256,512]{1,0:T(8,128)(2,1)S(1)}, u32[]{:S(2)}, u32[]{:S(2)}) %collective-permute-start.16) | collective-permute-done | bytes 262176 | tf_op jit(solution)/shard_map/ppermute | solution.py:57
  68.0 5.3 %collective-permute-done.18.refs_11_ = bf16[256,512]{1,0:T(8,128)(2,1)S(1)} collective-permute-done((bf16[256,512]{1,0:T(8,128)(2,1)}, bf16[256,512]{1,0:T(8,128)(2,1)S(1)}, u32[]{:S(2)}, u32[]{:S(2)}) %collective-permute-start.18) | collective-permute-done | bytes 262176 | tf_op jit(solution)/shard_map/ppermute | solution.py:57
  73.4 0.5 collective-permute-start.7
  73.9 3.3 %collective-permute-start.10 = (bf16[256,512]{1,0:T(8,128)(2,1)S(1)}, bf16[256,512]{1,0:T(8,128)(2,1)S(1)}, u32[]{:S(2)}, u32[]{:S(2)}) collective-permute-start(bf16[256,512]{1,0:T(8,128)(2,1)S(1)} %collective-permute-done.9.refs_7_), channel_id=1, source_target_pairs={{0,6},{1,7},{2,0},{3,1},{4,2},{5,3},{6,4},{7,5},{8,14},{9,15},{10,... | collective-permute-start | bytes 786440 | tf_op jit(solution)/shard_map/ppermute | solution.py:57
  77.2 1.0 fusion
  78.2 0.2 pad_maximum_fusion
  78.5 0.5 collective-permute-start.17
  79.1 8.8 %collective-permute-done.10.refs_3_ = bf16[256,512]{1,0:T(8,128)(2,1)S(1)} collective-permute-done((bf16[256,512]{1,0:T(8,128)(2,1)S(1)}, bf16[256,512]{1,0:T(8,128)(2,1)S(1)}, u32[]{:S(2)}, u32[]{:S(2)}) %collective-permute-start.10) | collective-permute-done | bytes 262176 | tf_op jit(solution)/shard_map/ppermute | solution.py:57
  87.9 0.5 collective-permute-start.8
  88.4 1.6 %copy-done.6 = bf16[4096,256]{1,0:T(8,128)(2,1)S(1)} copy-done((bf16[4096,256]{1,0:T(8,128)(2,1)S(1)}, bf16[4096,256]{1,0:T(8,128)(2,1)}, u32[]{:S(2)}) %copy-start.6) | copy-done | bytes 2097176
  90.0 1.6 %copy-done.7 = bf16[4096,256]{1,0:T(8,128)(2,1)S(1)} copy-done((bf16[4096,256]{1,0:T(8,128)(2,1)S(1)}, bf16[4096,256]{1,0:T(8,128)(2,1)}, u32[]{:S(2)}) %copy-start.7) | copy-done | bytes 2097176
  91.6 0.9 copy-done.9
  92.6 0.9 copy-done.11
  93.5 0.9 copy-done.13
  94.5 0.9 copy-done.15
  95.4 0.9 copy-done.17
  96.4 0.9 copy-done.19
  97.3 0.9 copy-done.21
  98.3 0.9 copy-done.23
  99.2 0.9 copy-done.25
  100.2 0.9 copy-done.27
  101.1 0.9 copy-done.29
  102.1 11.9 %project_retain.1 = (f32[512,512]{1,0:T(8,128)S(1)}, bf16[512,256]{1,0:T(8,128)(2,1)S(1)}, f32[512,128]{1,0:T(8,128)S(1)}) custom-call(s32[8]{0:T(128)S(1)} %stack.35.refs_0_, f32[2]{0:T(128)S(1)} %copy-done.30, bf16[256,512]{1,0:T(8,128)(2,1)S(1)} %get-tuple-element.26.refs_2_, bf16[256,512]{1,0:T(8,128)(2,1)S(1)} %copy-done.15, ...), custom_call_target="tpu_custom_call" | custom-call | flops 5905580032 | tf_op jit(solution)/shard_map/project_retain/pallas_call | solution.py:187
  114.1 3.4 %passage_near.1.refs_7_ = f32[512,512]{1,0:T(8,128)S(1)} custom-call(s32[8]{0:T(128)S(1)} %stack.35.refs_0_, bf16[256,512]{1,0:T(8,128)(2,1)S(1)} %bitcast.13, bf16[256,512]{1,0:T(8,128)(2,1)S(1)} %collective-permute-done.12.refs_2_, bf16[256,512]{1,0:T(8,128)(2,1)S(1)} %bitcast.17, bf16[256,512]{1,0:T(8,128)(2,1)S(1)} %collective-permute-done.13.refs_4_, ...), custom_call_target="tpu_custom_call" | custom-call | flops 1610612736 | tf_op jit(solution)/shard_map/passage_near/pallas_call | solution.py:322
  117.5 3.9 %passage_mix.1 = bf16[512,512]{1,0:T(8,128)(2,1)} custom-call(s32[8]{0:T(128)S(1)} %stack.35.refs_0_, bf16[256,512]{1,0:T(8,128)(2,1)S(1)} %collective-permute-done.7.refs_1_, bf16[256,512]{1,0:T(8,128)(2,1)S(1)} %collective-permute-done.8.refs_2_, bf16[256,512]{1,0:T(8,128)(2,1)S(1)} %collective-permute-done.10.refs_3_, ...), custom_call_target="tpu_custom_call" | custom-call | flops 536870912 | tf_op jit(solution)/shard_map/passage_mix/pallas_call | solution.py:376
  (98 shorter events, 1.1 us)
Async XLA Ops:
  1.1 25.3 %collective-permute-start.24 = (bf16[256,512]{1,0:T(8,128)(2,1)S(1)}, bf16[256,512]{1,0:T(8,128)(2,1)S(1)}, u32[]{:S(2)}, u32[]{:S(2)}) collective-permute-start(bf16[256,512]{1,0:T(8,128)(2,1)S(1)} %get-tuple-element.25.refs_4_), channel_id=1, source_target_pairs={{0,6},{1,7},{2,0},{3,1},{4,2},{5,3},{6,4},{7,5},{8,14},{9,15},{10,... | collective-permute-start | bytes 786440 | tf_op jit(solution)/shard_map/ppermute | solution.py:57
  6.2 21.9 %collective-permute-start.26 = (bf16[256,512]{1,0:T(8,128)(2,1)S(1)}, bf16[256,512]{1,0:T(8,128)(2,1)S(1)}, u32[]{:S(2)}, u32[]{:S(2)}) collective-permute-start(bf16[256,512]{1,0:T(8,128)(2,1)S(1)} %get-tuple-element.25.refs_4_), channel_id=1, source_target_pairs={{0,2},{1,3},{2,4},{3,5},{4,6},{5,7},{6,0},{7,1},{8,10},{9,11},{10,... | collective-permute-start | bytes 786440 | tf_op jit(solution)/shard_map/ppermute | solution.py:57
  6.2 17.7 %collective-permute-start.22 = (bf16[256,512]{1,0:T(8,128)(2,1)S(1)}, bf16[256,512]{1,0:T(8,128)(2,1)S(1)}, u32[]{:S(2)}, u32[]{:S(2)}) collective-permute-start(bf16[256,512]{1,0:T(8,128)(2,1)S(1)} %get-tuple-element.26.refs_2_), channel_id=1, source_target_pairs={{0,2},{1,3},{2,4},{3,5},{4,6},{5,7},{6,0},{7,1},{8,10},{9,11},{10,... | collective-permute-start | bytes 786440 | tf_op jit(solution)/shard_map/ppermute | solution.py:57
  7.3 12.1 %copy-start.35 = (s32[8]{0:T(128)}, s32[8]{0:T(128)S(1)}, u32[]{:S(2)}) copy-start(s32[8]{0:T(128)S(1)} %get-tuple-element.22.source) | copy-start | bytes 100
  7.9 3.6 %collective-permute-start = (s32[4]{0:T(128)S(1)}, s32[4]{0:T(128)S(1)}, u32[]{:S(2)}, u32[]{:S(2)}) collective-permute-start(s32[4]{0:T(128)S(1)} %get-tuple-element.30), channel_id=1, source_target_pairs={{0,8},{8,0},{16,24},{24,16},{1,9},{9,1},{17,25},{25,17},{2,10},{10... | collective-permute-start | bytes 56 | tf_op jit(solution)/shard_map/ppermute | solution.py:414
  9.4 4.5 %collective-permute-start.1 = (s32[4]{0:T(128)S(1)}, s32[4]{0:T(128)S(1)}, u32[]{:S(2)}, u32[]{:S(2)}) collective-permute-start(s32[4]{0:T(128)S(1)} %get-tuple-element.32), channel_id=1, source_target_pairs={{0,16},{8,24},{16,0},{24,8},{1,17},{9,25},{17,1},{25,9},{2,18},{10... | collective-permute-start | bytes 56 | tf_op jit(solution)/shard_map/ppermute | solution.py:414
  11.5 4.5 %collective-permute-start.2 = (s32[4]{0:T(128)S(1)}, s32[4]{0:T(128)S(1)}, u32[]{:S(2)}, u32[]{:S(2)}) collective-permute-start(s32[4]{0:T(128)S(1)} %get-tuple-element.31), channel_id=1, source_target_pairs={{0,24},{8,16},{16,8},{24,0},{1,25},{9,17},{17,9},{25,1},{2,26},{10... | collective-permute-start | bytes 56 | tf_op jit(solution)/shard_map/ppermute | solution.py:414
  19.4 8.7 %collective-permute-start.3 = (bf16[4,64,512]{2,1,0:T(8,128)(2,1)}, bf16[4,64,512]{2,1,0:T(8,128)(2,1)S(1)}, u32[]{:S(2)}, u32[]{:S(2)}) collective-permute-start(bf16[4,64,512]{2,1,0:T(8,128)(2,1)} %get-tuple-element.13), channel_id=1, source_target_pairs={{0,8},{8,0},{16,24},{24,16},{1,9},{9,1},{17,25},{25,17},{2,10},{10... | collective-permute-start | bytes 786440 | tf_op jit(solution)/shard_map/ppermute | solution.py:414
  21.0 12.2 %collective-permute-start.4 = (bf16[4,64,512]{2,1,0:T(8,128)(2,1)}, bf16[4,64,512]{2,1,0:T(8,128)(2,1)S(1)}, u32[]{:S(2)}, u32[]{:S(2)}) collective-permute-start(bf16[4,64,512]{2,1,0:T(8,128)(2,1)} %get-tuple-element.14), channel_id=1, source_target_pairs={{0,16},{8,24},{16,0},{24,8},{1,17},{9,25},{17,1},{25,9},{2,18},{10... | collective-permute-start | bytes 786440 | tf_op jit(solution)/shard_map/ppermute | solution.py:414
  23.9 15.9 %copy-start.10 = (bf16[256,512]{1,0:T(8,128)(2,1)}, bf16[256,512]{1,0:T(8,128)(2,1)S(1)}, u32[]{:S(2)}) copy-start(bf16[256,512]{1,0:T(8,128)(2,1)S(1)} %collective-permute-done.22.refs_6_) | copy-start | bytes 786436
  23.9 10.9 %collective-permute-start.5 = (bf16[4,64,512]{2,1,0:T(8,128)(2,1)}, bf16[4,64,512]{2,1,0:T(8,128)(2,1)S(1)}, u32[]{:S(2)}, u32[]{:S(2)}) collective-permute-start(bf16[4,64,512]{2,1,0:T(8,128)(2,1)} %get-tuple-element.15), channel_id=1, source_target_pairs={{0,24},{8,16},{16,8},{24,0},{1,25},{9,17},{17,9},{25,1},{2,26},{10... | collective-permute-start | bytes 786440 | tf_op jit(solution)/shard_map/ppermute | solution.py:414
  26.4 13.5 %collective-permute-start.28 = (bf16[256,512]{1,0:T(8,128)(2,1)S(1)}, bf16[256,512]{1,0:T(8,128)(2,1)S(1)}, u32[]{:S(2)}, u32[]{:S(2)}) collective-permute-start(bf16[256,512]{1,0:T(8,128)(2,1)S(1)} %get-tuple-element.26.refs_2_), channel_id=1, source_target_pairs={{0,6},{1,7},{2,0},{3,1},{4,2},{5,3},{6,4},{7,5},{8,14},{9,15},{10,... | collective-permute-start | bytes 786440 | tf_op jit(solution)/shard_map/ppermute | solution.py:57
  28.1 13.0 %copy-start.8 = (bf16[256,512]{1,0:T(8,128)(2,1)}, bf16[256,512]{1,0:T(8,128)(2,1)S(1)}, u32[]{:S(2)}) copy-start(bf16[256,512]{1,0:T(8,128)(2,1)S(1)} %collective-permute-done.26.refs_10_) | copy-start | bytes 786436
  28.1 11.8 %collective-permute-start.20 = (bf16[256,512]{1,0:T(8,128)(2,1)S(1)}, bf16[256,512]{1,0:T(8,128)(2,1)S(1)}, u32[]{:S(2)}, u32[]{:S(2)}) collective-permute-start(bf16[256,512]{1,0:T(8,128)(2,1)S(1)} %get-tuple-element.26.refs_2_), channel_id=1, source_target_pairs={{0,1},{1,0},{2,3},{3,2},{4,5},{5,4},{6,7},{7,6},{8,9},{9,8},{10,11... | collective-permute-start | bytes 786440 | tf_op jit(solution)/shard_map/ppermute | solution.py:61
  28.1 8.9 %copy-start.31 = (bf16[4,64,512]{2,1,0:T(8,128)(2,1)}, bf16[4,64,512]{2,1,0:T(8,128)(2,1)S(1)}, u32[]{:S(2)}) copy-start(bf16[4,64,512]{2,1,0:T(8,128)(2,1)S(1)} %collective-permute-done.3.refs_0_) | copy-start | bytes 786436
  28.1 13.0 %collective-permute-start.21 = (bf16[256,512]{1,0:T(8,128)(2,1)S(1)}, bf16[256,512]{1,0:T(8,128)(2,1)S(1)}, u32[]{:S(2)}, u32[]{:S(2)}) collective-permute-start(bf16[256,512]{1,0:T(8,128)(2,1)S(1)} %get-tuple-element.25.refs_4_), channel_id=1, source_target_pairs={{0,1},{1,0},{2,3},{3,2},{4,5},{5,4},{6,7},{7,6},{8,9},{9,8},{10,11... | collective-permute-start | bytes 786440 | tf_op jit(solution)/shard_map/ppermute | solution.py:61
  33.2 3.8 %copy-start.32 = (bf16[4,64,512]{2,1,0:T(8,128)(2,1)}, bf16[4,64,512]{2,1,0:T(8,128)(2,1)S(1)}, u32[]{:S(2)}) copy-start(bf16[4,64,512]{2,1,0:T(8,128)(2,1)S(1)} %collective-permute-done.4.refs_1_) | copy-start | bytes 786436
  33.2 8.6 %collective-permute-start.30 = (bf16[256,512]{1,0:T(8,128)(2,1)S(1)}, bf16[256,512]{1,0:T(8,128)(2,1)S(1)}, u32[]{:S(2)}, u32[]{:S(2)}) collective-permute-start(bf16[256,512]{1,0:T(8,128)(2,1)S(1)} %collective-permute-done.22.refs_6_), channel_id=1, source_target_pairs={{0,2},{1,3},{2,4},{3,5},{4,6},{5,7},{6,0},{7,1},{8,10},{9,11},{10,... | collective-permute-start | bytes 786440 | tf_op jit(solution)/shard_map/ppermute | solution.py:57
  34.8 2.3 %copy-start.33 = (bf16[4,64,512]{2,1,0:T(8,128)(2,1)}, bf16[4,64,512]{2,1,0:T(8,128)(2,1)S(1)}, u32[]{:S(2)}) copy-start(bf16[4,64,512]{2,1,0:T(8,128)(2,1)S(1)} %collective-permute-done.5.refs_2_) | copy-start | bytes 786436
  34.8 9.7 %collective-permute-start.32 = (bf16[256,512]{1,0:T(8,128)(2,1)S(1)}, bf16[256,512]{1,0:T(8,128)(2,1)S(1)}, u32[]{:S(2)}, u32[]{:S(2)}) collective-permute-start(bf16[256,512]{1,0:T(8,128)(2,1)S(1)} %collective-permute-done.24.refs_8_), channel_id=1, source_target_pairs={{0,6},{1,7},{2,0},{3,1},{4,2},{5,3},{6,4},{7,5},{8,14},{9,15},{10,... | collective-permute-start | bytes 786440 | tf_op jit(solution)/shard_map/ppermute | solution.py:57
  37.0 19.7 %copy-start.34 = (bf16[4096,2]{0,1:T(2,128)(2,1)S(1)}, bf16[4096,2]{0,1:T(2,128)(2,1)}, u32[]{:S(2)}) copy-start(bf16[4096,2]{0,1:T(2,128)(2,1)} %param.19) | copy-start | bytes 49156
  39.8 7.2 %collective-permute-start.23 = (bf16[256,512]{1,0:T(8,128)(2,1)S(1)}, bf16[256,512]{1,0:T(8,128)(2,1)S(1)}, u32[]{:S(2)}, u32[]{:S(2)}) collective-permute-start(bf16[256,512]{1,0:T(8,128)(2,1)S(1)} %collective-permute-done.22.refs_6_), channel_id=1, source_target_pairs={{0,1},{1,0},{2,3},{3,2},{4,5},{5,4},{6,7},{7,6},{8,9},{9,8},{10,11... | collective-permute-start | bytes 786440 | tf_op jit(solution)/shard_map/ppermute | solution.py:61
  40.6 9.4 %collective-permute-start.25 = (bf16[256,512]{1,0:T(8,128)(2,1)S(1)}, bf16[256,512]{1,0:T(8,128)(2,1)S(1)}, u32[]{:S(2)}, u32[]{:S(2)}) collective-permute-start(bf16[256,512]{1,0:T(8,128)(2,1)S(1)} %collective-permute-done.24.refs_8_), channel_id=1, source_target_pairs={{0,1},{1,0},{2,3},{3,2},{4,5},{5,4},{6,7},{7,6},{8,9},{9,8},{10,11... | collective-permute-start | bytes 786440 | tf_op jit(solution)/shard_map/ppermute | solution.py:61
  41.8 9.1 %collective-permute-start.27 = (bf16[256,512]{1,0:T(8,128)(2,1)S(1)}, bf16[256,512]{1,0:T(8,128)(2,1)S(1)}, u32[]{:S(2)}, u32[]{:S(2)}) collective-permute-start(bf16[256,512]{1,0:T(8,128)(2,1)S(1)} %collective-permute-done.26.refs_10_), channel_id=1, source_target_pairs={{0,1},{1,0},{2,3},{3,2},{4,5},{5,4},{6,7},{7,6},{8,9},{9,8},{10,11... | collective-permute-start | bytes 786440 | tf_op jit(solution)/shard_map/ppermute | solution.py:61
  41.9 14.1 %copy-start.18 = (bf16[256,512]{1,0:T(8,128)(2,1)}, bf16[256,512]{1,0:T(8,128)(2,1)S(1)}, u32[]{:S(2)}) copy-start(bf16[256,512]{1,0:T(8,128)(2,1)S(1)} %collective-permute-done.30.refs_14_) | copy-start | bytes 786436
  41.9 13.4 %collective-permute-start.29 = (bf16[256,512]{1,0:T(8,128)(2,1)S(1)}, bf16[256,512]{1,0:T(8,128)(2,1)S(1)}, u32[]{:S(2)}, u32[]{:S(2)}) collective-permute-start(bf16[256,512]{1,0:T(8,128)(2,1)S(1)} %collective-permute-done.28.refs_12_), channel_id=1, source_target_pairs={{0,1},{1,0},{2,3},{3,2},{4,5},{5,4},{6,7},{7,6},{8,9},{9,8},{10,11... | collective-permute-start | bytes 786440 | tf_op jit(solution)/shard_map/ppermute | solution.py:61
  44.5 12.2 %copy-start.20 = (bf16[256,512]{1,0:T(8,128)(2,1)}, bf16[256,512]{1,0:T(8,128)(2,1)S(1)}, u32[]{:S(2)}) copy-start(bf16[256,512]{1,0:T(8,128)(2,1)S(1)} %collective-permute-done.32.refs_16_) | copy-start | bytes 786436
  44.5 12.2 %collective-permute-start.6 = (bf16[256,512]{1,0:T(8,128)(2,1)}, bf16[256,512]{1,0:T(8,128)(2,1)S(1)}, u32[]{:S(2)}, u32[]{:S(2)}) collective-permute-start(bf16[256,512]{1,0:T(8,128)(2,1)} %bitcast.10), channel_id=1, source_target_pairs={{0,2},{1,3},{2,4},{3,5},{4,6},{5,7},{6,0},{7,1},{8,10},{9,11},{10,... | collective-permute-start | bytes 786440 | tf_op jit(solution)/shard_map/ppermute | solution.py:57
  47.8 14.5 %collective-permute-start.9 = (bf16[256,512]{1,0:T(8,128)(2,1)}, bf16[256,512]{1,0:T(8,128)(2,1)S(1)}, u32[]{:S(2)}, u32[]{:S(2)}) collective-permute-start(bf16[256,512]{1,0:T(8,128)(2,1)} %bitcast.14), channel_id=1, source_target_pairs={{0,6},{1,7},{2,0},{3,1},{4,2},{5,3},{6,4},{7,5},{8,14},{9,15},{10,... | collective-permute-start | bytes 786440 | tf_op jit(solution)/shard_map/ppermute | solution.py:57
  50.7 17.2 %collective-permute-start.16 = (bf16[256,512]{1,0:T(8,128)(2,1)}, bf16[256,512]{1,0:T(8,128)(2,1)S(1)}, u32[]{:S(2)}, u32[]{:S(2)}) collective-permute-start(bf16[256,512]{1,0:T(8,128)(2,1)} %bitcast.15), channel_id=1, source_target_pairs={{0,2},{1,3},{2,4},{3,5},{4,6},{5,7},{6,0},{7,1},{8,10},{9,11},{10,... | collective-permute-start | bytes 786440 | tf_op jit(solution)/shard_map/ppermute | solution.py:57
  51.6 21.7 %collective-permute-start.18 = (bf16[256,512]{1,0:T(8,128)(2,1)}, bf16[256,512]{1,0:T(8,128)(2,1)S(1)}, u32[]{:S(2)}, u32[]{:S(2)}) collective-permute-start(bf16[256,512]{1,0:T(8,128)(2,1)} %bitcast.11), channel_id=1, source_target_pairs={{0,6},{1,7},{2,0},{3,1},{4,2},{5,3},{6,4},{7,5},{8,14},{9,15},{10,... | collective-permute-start | bytes 786440 | tf_op jit(solution)/shard_map/ppermute | solution.py:57
  55.3 0.7 copy-start.28
  56.0 17.4 %collective-permute-start.12 = (bf16[256,512]{1,0:T(8,128)(2,1)}, bf16[256,512]{1,0:T(8,128)(2,1)S(1)}, u32[]{:S(2)}, u32[]{:S(2)}) collective-permute-start(bf16[256,512]{1,0:T(8,128)(2,1)} %bitcast.12), channel_id=1, source_target_pairs={{0,1},{1,0},{2,3},{3,2},{4,5},{5,4},{6,7},{7,6},{8,9},{9,8},{10,11... | collective-permute-start | bytes 786440 | tf_op jit(solution)/shard_map/ppermute | solution.py:61
  56.7 17.2 %collective-permute-start.13 = (bf16[256,512]{1,0:T(8,128)(2,1)}, bf16[256,512]{1,0:T(8,128)(2,1)S(1)}, u32[]{:S(2)}, u32[]{:S(2)}) collective-permute-start(bf16[256,512]{1,0:T(8,128)(2,1)} %bitcast.16), channel_id=1, source_target_pairs={{0,1},{1,0},{2,3},{3,2},{4,5},{5,4},{6,7},{7,6},{8,9},{9,8},{10,11... | collective-permute-start | bytes 786440 | tf_op jit(solution)/shard_map/ppermute | solution.py:61
  58.1 30.3 %copy-start.30 = (f32[2]{0:T(128)S(1)}, f32[2]{0:T(128)}, u32[]{:S(2)}) copy-start(f32[2]{0:T(128)} %refs_1_.1) | copy-start | bytes 28
  59.7 28.8 %copy-start.5 = (bf16[4096,256]{1,0:T(8,128)(2,1)S(1)}, bf16[4096,256]{1,0:T(8,128)(2,1)}, u32[]{:S(2)}) copy-start(bf16[4096,256]{1,0:T(8,128)(2,1)} %refs_18_.1) | copy-start | bytes 6291460
  62.3 16.1 %collective-permute-start.31 = (bf16[256,512]{1,0:T(8,128)(2,1)}, bf16[256,512]{1,0:T(8,128)(2,1)S(1)}, u32[]{:S(2)}, u32[]{:S(2)}) collective-permute-start(bf16[256,512]{1,0:T(8,128)(2,1)} %copy-done.18), channel_id=1, source_target_pairs={{0,1},{1,0},{2,3},{3,2},{4,5},{5,4},{6,7},{7,6},{8,9},{9,8},{10,11... | collective-permute-start | bytes 786440 | tf_op jit(solution)/shard_map/ppermute | solution.py:61
  68.0 10.5 %collective-permute-start.33 = (bf16[256,512]{1,0:T(8,128)(2,1)}, bf16[256,512]{1,0:T(8,128)(2,1)S(1)}, u32[]{:S(2)}, u32[]{:S(2)}) collective-permute-start(bf16[256,512]{1,0:T(8,128)(2,1)} %copy-done.20), channel_id=1, source_target_pairs={{0,1},{1,0},{2,3},{3,2},{4,5},{5,4},{6,7},{7,6},{8,9},{9,8},{10,11... | collective-permute-start | bytes 786440 | tf_op jit(solution)/shard_map/ppermute | solution.py:61
  73.3 5.7 %collective-permute-start.14 = (bf16[256,512]{1,0:T(8,128)(2,1)S(1)}, bf16[256,512]{1,0:T(8,128)(2,1)S(1)}, u32[]{:S(2)}, u32[]{:S(2)}) collective-permute-start(bf16[256,512]{1,0:T(8,128)(2,1)S(1)} %collective-permute-done.6.refs_5_), channel_id=1, source_target_pairs={{0,1},{1,0},{2,3},{3,2},{4,5},{5,4},{6,7},{7,6},{8,9},{9,8},{10,11... | collective-permute-start | bytes 786440 | tf_op jit(solution)/shard_map/ppermute | solution.py:61
  73.4 14.6 %collective-permute-start.7 = (bf16[256,512]{1,0:T(8,128)(2,1)S(1)}, bf16[256,512]{1,0:T(8,128)(2,1)S(1)}, u32[]{:S(2)}, u32[]{:S(2)}) collective-permute-start(bf16[256,512]{1,0:T(8,128)(2,1)S(1)} %collective-permute-done.6.refs_5_), channel_id=1, source_target_pairs={{0,2},{1,3},{2,4},{3,5},{4,6},{5,7},{6,0},{7,1},{8,10},{9,11},{10,... | collective-permute-start | bytes 786440 | tf_op jit(solution)/shard_map/ppermute | solution.py:57
  73.9 14.0 %collective-permute-start.10 = (bf16[256,512]{1,0:T(8,128)(2,1)S(1)}, bf16[256,512]{1,0:T(8,128)(2,1)S(1)}, u32[]{:S(2)}, u32[]{:S(2)}) collective-permute-start(bf16[256,512]{1,0:T(8,128)(2,1)S(1)} %collective-permute-done.9.refs_7_), channel_id=1, source_target_pairs={{0,6},{1,7},{2,0},{3,1},{4,2},{5,3},{6,4},{7,5},{8,14},{9,15},{10,... | collective-permute-start | bytes 786440 | tf_op jit(solution)/shard_map/ppermute | solution.py:57
  78.4 35.6 %collective-permute-start.15 = (bf16[256,512]{1,0:T(8,128)(2,1)S(1)}, bf16[256,512]{1,0:T(8,128)(2,1)S(1)}, u32[]{:S(2)}, u32[]{:S(2)}) collective-permute-start(bf16[256,512]{1,0:T(8,128)(2,1)S(1)} %collective-permute-done.9.refs_7_), channel_id=1, source_target_pairs={{0,1},{1,0},{2,3},{3,2},{4,5},{5,4},{6,7},{7,6},{8,9},{9,8},{10,11... | collective-permute-start | bytes 786440 | tf_op jit(solution)/shard_map/ppermute | solution.py:61
  78.5 35.5 %collective-permute-start.17 = (bf16[256,512]{1,0:T(8,128)(2,1)S(1)}, bf16[256,512]{1,0:T(8,128)(2,1)S(1)}, u32[]{:S(2)}, u32[]{:S(2)}) collective-permute-start(bf16[256,512]{1,0:T(8,128)(2,1)S(1)} %collective-permute-done.16.refs_9_), channel_id=1, source_target_pairs={{0,1},{1,0},{2,3},{3,2},{4,5},{5,4},{6,7},{7,6},{8,9},{9,8},{10,11... | collective-permute-start | bytes 786440 | tf_op jit(solution)/shard_map/ppermute | solution.py:61
  79.0 35.0 %collective-permute-start.19 = (bf16[256,512]{1,0:T(8,128)(2,1)S(1)}, bf16[256,512]{1,0:T(8,128)(2,1)S(1)}, u32[]{:S(2)}, u32[]{:S(2)}) collective-permute-start(bf16[256,512]{1,0:T(8,128)(2,1)S(1)} %collective-permute-done.18.refs_11_), channel_id=1, source_target_pairs={{0,1},{1,0},{2,3},{3,2},{4,5},{5,4},{6,7},{7,6},{8,9},{9,8},{10,11... | collective-permute-start | bytes 786440 | tf_op jit(solution)/shard_map/ppermute | solution.py:61
  87.9 29.5 %collective-permute-start.11 = (bf16[256,512]{1,0:T(8,128)(2,1)S(1)}, bf16[256,512]{1,0:T(8,128)(2,1)S(1)}, u32[]{:S(2)}, u32[]{:S(2)}) collective-permute-start(bf16[256,512]{1,0:T(8,128)(2,1)S(1)} %collective-permute-done.10.refs_3_), channel_id=1, source_target_pairs={{0,1},{1,0},{2,3},{3,2},{4,5},{5,4},{6,7},{7,6},{8,9},{9,8},{10,11... | collective-permute-start | bytes 786440 | tf_op jit(solution)/shard_map/ppermute | solution.py:61
  87.9 29.5 %collective-permute-start.8 = (bf16[256,512]{1,0:T(8,128)(2,1)S(1)}, bf16[256,512]{1,0:T(8,128)(2,1)S(1)}, u32[]{:S(2)}, u32[]{:S(2)}) collective-permute-start(bf16[256,512]{1,0:T(8,128)(2,1)S(1)} %collective-permute-done.7.refs_1_), channel_id=1, source_target_pairs={{0,1},{1,0},{2,3},{3,2},{4,5},{5,4},{6,7},{7,6},{8,9},{9,8},{10,11... | collective-permute-start | bytes 786440 | tf_op jit(solution)/shard_map/ppermute | solution.py:61
  88.4 1.6 %copy-start.6 = (bf16[4096,256]{1,0:T(8,128)(2,1)S(1)}, bf16[4096,256]{1,0:T(8,128)(2,1)}, u32[]{:S(2)}) copy-start(bf16[4096,256]{1,0:T(8,128)(2,1)} %refs_19_.1) | copy-start | bytes 6291460
  90.0 1.6 %copy-start.7 = (bf16[4096,256]{1,0:T(8,128)(2,1)S(1)}, bf16[4096,256]{1,0:T(8,128)(2,1)}, u32[]{:S(2)}) copy-start(bf16[4096,256]{1,0:T(8,128)(2,1)} %refs_21_.1) | copy-start | bytes 6291460
  91.6 0.9 copy-start.9
  92.6 0.9 copy-start.11
  93.5 0.9 copy-start.13
  94.5 0.9 copy-start.15
  95.4 0.9 copy-start.17
  96.4 0.9 copy-start.19
  97.3 0.9 copy-start.21
  98.3 0.9 copy-start.23
  99.2 0.9 copy-start.25
  100.2 0.9 copy-start.27
  101.1 0.9 copy-start.29
  102.1 11.9 %copy-start = (bf16[4096,256]{1,0:T(8,128)(2,1)S(1)}, bf16[4096,256]{1,0:T(8,128)(2,1)}, u32[]{:S(2)}) copy-start(bf16[4096,256]{1,0:T(8,128)(2,1)} %refs_5_.1) | copy-start | bytes 6291460
  102.1 12.0 %copy-start.1 = (bf16[4096,256]{1,0:T(8,128)(2,1)S(1)}, bf16[4096,256]{1,0:T(8,128)(2,1)}, u32[]{:S(2)}) copy-start(bf16[4096,256]{1,0:T(8,128)(2,1)} %refs_6_.1) | copy-start | bytes 6291460
  102.1 12.0 %copy-start.2 = (bf16[4,64,512]{2,1,0:T(8,128)(2,1)S(1)}, bf16[4,64,512]{2,1,0:T(8,128)(2,1)}, u32[]{:S(2)}) copy-start(bf16[4,64,512]{2,1,0:T(8,128)(2,1)} %get-tuple-element.16) | copy-start | bytes 786436
  102.1 12.0 %copy-start.3 = (bf16[4,64,512]{2,1,0:T(8,128)(2,1)S(1)}, bf16[4,64,512]{2,1,0:T(8,128)(2,1)}, u32[]{:S(2)}) copy-start(bf16[4,64,512]{2,1,0:T(8,128)(2,1)} %get-tuple-element.17) | copy-start | bytes 786436
  114.0 3.5 %copy-start.4 = (bf16[2,128,256]{2,1,0:T(8,128)(2,1)S(1)}, bf16[2,128,256]{2,1,0:T(8,128)(2,1)}, u32[]{:S(2)}) copy-start(bf16[2,128,256]{2,1,0:T(8,128)(2,1)} %refs_11_.1) | copy-start | bytes 393220
  (6 other events, 4.2 us)
